TPU v7x, 256 devices: a whole 4x4x8 slice. The times are simulated.
256 devices in a mesh: sp: 16 (over y, x), tp: 16 (over z, core).
Axes of the slice: x: 4, y: 4, z: 8, core: 2. Of those that a mesh axis runs over, the one named last changes fastest.
Arguments:
- lru_input: bfloat16 [4096, 2048], P('sp', 'tp'), may hold values from -27 to 27
- gate_input: bfloat16 [4096, 2048], P('sp', 'tp'), may hold values from -6 to 6
- documents: int32 [4096], P('sp'), may hold values from 0 to 3, never falling along the last dimension, each value on 1 to 1536 neighbouring positions
- conv_taps: bfloat16 [4, 2048], P(None, 'tp'), may hold values from -3 to 3
- rate_weight: bfloat16 [16, 128, 128], P('tp'), may hold values from -0.5 to 0.5
- inlet_weight: bfloat16 [16, 128, 128], P('tp'), may hold values from -0.5 to 0.5
- decay_param: float32 [2048], P('tp')
- lru_gain: float32 [2048], P('tp'), may hold values from 0.1 to 1.9
- out_weight: bfloat16 [2048, 2048], P('tp'), may hold values from -0.125 to 0.125
- residual: bfloat16 [4096, 2048], P('sp'), may hold values from -6 to 6
- ffn_gain: float32 [2048], replicated, may hold values from 0.1 to 1.9
- routes: int32 [4096, 2], P('sp'), may hold values from 0 to 15, all different within a row; in each aligned block of 16 rows (0 to 15, 16 to 31, ...) at most 4 rows name the same one
- route_weights: float32 [4096, 2], P('sp'), may hold values from 0.1 to 0.9
- w_gate: bfloat16 [16, 2048, 6144], P('sp', None, 'tp'), may hold values from -0.125 to 0.125
- w_up: bfloat16 [16, 2048, 6144], P('sp', None, 'tp'), may hold values from -0.125 to 0.125
- w_down: bfloat16 [16, 6144, 2048], P('sp', 'tp'), may hold values from -0.078125 to 0.078125
Outputs:
- mixed_out: bfloat16 [4096, 2048], P(('sp', 'tp'))
Inputs may be any that keep to these rules, and one draw needn't show every extreme that they name: `documents`: document numbers start at 0 and never fall along the sequence; a document spans at most 1536 positions. `routes`: each row names 2 different experts. In each aligned block of 16 rows no expert is named by more than 4 rows, a bound that some block reaches.
All inputs are finite; a program needn't handle non-finite values.
Results may differ from a plain program's by a relative error of at most 0.017.
Values may be sent and summed in bfloat16 or wider, within the bound.
A program may use at most 64 MiB of HBM per device.

v0:
```python
import jax
import jax.numpy as jnp
from jax import lax
from jax.sharding import PartitionSpec as P

D_RNN = 2048


EPSILON = 1e-06
RATE_SCALE = 8.0


def shifted(block, axis, distance):
    devices = range(lax.axis_size(axis))
    route = [(i - distance, i) for i in devices if i - distance in devices]
    return lax.ppermute(block, axis, route)


def sent_to_all(x, axis):
    devices = lax.axis_size(axis)
    return lax.all_to_all(jnp.broadcast_to(x[None], (devices, *x.shape)), axis, 0, 0, tiled=True)


def collected_together(x, axis):
    leaves = jax.tree.leaves(x)
    sequence = sorted(range(len(leaves)), key=lambda k: -leaves[k].size)
    width = (1, *leaves[sequence[0]].shape)[-1]
    lines = [
        jnp.pad(leaves[k].reshape(-1), (0, -leaves[k].size % width)).reshape(-1, width)
        for k in sequence
    ]
    both, at, found = (sent_to_all(jnp.concatenate(lines), axis), 0, {})
    for k, line in zip(sequence, lines):
        section = both[:, at : at + len(line)].reshape(len(both), -1)
        found[k] = section[:, : leaves[k].size].reshape(-1, *leaves[k].shape)
        at += len(line)
    numbers = iter(range(len(leaves)))
    return jax.tree.map(lambda _: found[next(numbers)], x)


def folded_in_pairs(pieces, combine):
    while len(jax.tree.leaves(pieces)[0]) > 1:
        pieces = jax.vmap(combine)(
            *(jax.tree.map(lambda part: part[side::2], pieces) for side in (0, 1))
        )
    return jax.tree.map(lambda part: part[0], pieces)


def carried_in(x, axis, combine, identity):
    devices, here = (lax.axis_size(axis), lax.axis_index(axis))
    passed = jnp.arange(devices) < here

    def kept(part, zero, own):
        part = jnp.where(
            passed.reshape(-1, *(1 for _ in own.shape)), part, jnp.asarray(zero, own.dtype)
        )
        return part

    pieces = collected_together(x, axis)
    return folded_in_pairs(jax.tree.map(kept, pieces, identity, x), combine)


def of_everyone(x, axis):
    return sent_to_all(x, axis).sum(axis=0)


def in_blocks(x, dim, devices):
    shape = x.shape
    parts = x.reshape(*shape[:dim], devices, shape[dim] // devices, *shape[dim + 1 :])
    return jnp.moveaxis(parts, dim, 0)


def summed_on_arrival(x, axis, dim):
    parts = in_blocks(x, dim, lax.axis_size(axis))
    arrived = lax.all_to_all(parts, axis, split_axis=0, concat_axis=0, tiled=True)
    return arrived.astype(jnp.float32).sum(axis=0)


def join_runs(earlier_run, later_run):
    return (earlier_run[0] * later_run[0], later_run[0] * earlier_run[1] + later_run[1])


def slot_targets(route_block, expert_count, capacity):
    flat_routes = route_block.reshape(-1)
    onehot = (flat_routes[:, None] == jnp.arange(expert_count, dtype=jnp.int32)[None, :]).astype(
        jnp.int32
    )
    earlier_hits = jnp.cumsum(onehot, axis=0) - onehot
    slot_index = jnp.sum(earlier_hits * onehot, axis=1)
    return (flat_routes * capacity + slot_index).reshape(route_block.shape)


def pick_matrix(targets, slot_total):
    slot_hits = targets[None, :, :] == jnp.arange(slot_total, dtype=jnp.int32)[:, None, None]
    return jnp.sum(slot_hits.astype(jnp.int32), axis=2).astype(jnp.bfloat16)


def rms_rows(row_block, gain_vector):
    floated = row_block.astype(jnp.float32)
    inverse_rms = lax.rsqrt(jnp.mean(floated * floated, axis=1, keepdims=True) + EPSILON)
    return (floated * inverse_rms * gain_vector[None, :]).astype(jnp.bfloat16)


def expert_apply(row_piece, gate_weight, up_weight, down_weight):
    gate_part = jnp.dot(row_piece, gate_weight, preferred_element_type=jnp.float32)
    up_part = jnp.dot(row_piece, up_weight, preferred_element_type=jnp.float32)
    hidden_units = (jax.nn.silu(gate_part) * up_part).astype(jnp.bfloat16)
    return jnp.dot(hidden_units, down_weight, preferred_element_type=jnp.float32)


def local(
    lru_input,
    gate_input,
    documents,
    conv_taps,
    rate_weight,
    inlet_weight,
    decay_param,
    lru_gain,
    out_weight,
    residual,
    ffn_gain,
    routes,
    route_weights,
    w_gate,
    w_up,
    w_down,
):
    positions = lru_input.shape[0]
    channels = lru_input.shape[1]
    model_width = residual.shape[1]
    reach_back = conv_taps.shape[0] - 1
    tail_rows, tail_docs = shifted(
        (lru_input[positions - reach_back :], documents[positions - reach_back :] + 1), "sp", 1
    )
    prior_docs = jnp.concatenate([tail_docs - 1, documents])
    padded_input = jnp.concatenate([tail_rows, lru_input], axis=0)
    conv_sum = jnp.zeros((positions, channels), jnp.float32)
    for tap_index in range(reach_back + 1):
        same_doc = (prior_docs[tap_index : tap_index + positions] == documents).astype(jnp.float32)[
            :, None
        ]
        conv_sum = (
            conv_sum
            + padded_input[tap_index : tap_index + positions].astype(jnp.float32)
            * conv_taps[tap_index].astype(jnp.float32)[None, :]
            * same_doc
        )
    convolved = conv_sum.astype(jnp.bfloat16)
    grouped = convolved.reshape(positions, rate_weight.shape[0], rate_weight.shape[1])
    rate_gate = jax.nn.sigmoid(
        jnp.einsum(
            "tnc,ncd->tnd", grouped, rate_weight, preferred_element_type=jnp.float32
        ).reshape(positions, channels)
    )
    inlet_gate = jax.nn.sigmoid(
        jnp.einsum(
            "tnc,ncd->tnd", grouped, inlet_weight, preferred_element_type=jnp.float32
        ).reshape(positions, channels)
    )
    log_decay = -RATE_SCALE * rate_gate * jax.nn.softplus(-decay_param)[None, :]
    starts = (prior_docs[reach_back - 1 : reach_back - 1 + positions] != documents)[:, None]
    decay_step = jnp.where(starts, 0.0, jnp.exp(log_decay))
    norm_factor = jnp.where(starts, 1.0, jnp.sqrt(-jnp.expm1(2.0 * log_decay)))
    drive_term = norm_factor * inlet_gate * convolved.astype(jnp.float32)
    decay_run, local_state = lax.associative_scan(join_runs, (decay_step, drive_term), axis=0)
    carried = carried_in(
        (decay_run[positions - 1], local_state[positions - 1]),
        "sp",
        join_runs,
        (jnp.ones((channels,), jnp.float32), jnp.zeros((channels,), jnp.float32)),
    )
    hidden_state = local_state + decay_run * carried[1][None, :]
    square_sums = of_everyone(jnp.sum(hidden_state * hidden_state, axis=1), "tp")
    inverse_rms = lax.rsqrt(square_sums[:, None] / D_RNN + EPSILON)
    mixer_rows = (
        hidden_state * inverse_rms * lru_gain[None, :] * jax.nn.gelu(gate_input.astype(jnp.float32))
    ).astype(jnp.bfloat16)
    tp_count = lax.axis_size("tp")
    tp_here = lax.axis_index("tp")
    expert_count = lax.axis_size("sp")
    route_rows = positions // tp_count
    top_count = routes.shape[1]
    capacity = 2 * top_count * route_rows // expert_count
    slot_total = expert_count * capacity
    projected = summed_on_arrival(
        jnp.dot(mixer_rows, out_weight, preferred_element_type=jnp.float32).astype(jnp.bfloat16),
        "tp",
        0,
    )
    own_rows = (
        lax.dynamic_slice_in_dim(residual, tp_here * route_rows, route_rows, 0).astype(jnp.float32)
        + projected
    ).astype(jnp.bfloat16)
    own_routes = lax.dynamic_slice_in_dim(routes, tp_here * route_rows, route_rows, 0)
    targets = slot_targets(own_routes, expert_count, capacity)
    outgoing = jnp.dot(
        pick_matrix(targets, slot_total),
        rms_rows(own_rows, ffn_gain),
        preferred_element_type=jnp.float32,
    ).astype(jnp.bfloat16)
    arrived = lax.all_to_all(
        outgoing.reshape(expert_count, capacity, model_width),
        "sp",
        split_axis=0,
        concat_axis=0,
        tiled=True,
    )
    partial_out = expert_apply(
        lax.all_gather(arrived.reshape(slot_total, model_width), "tp", axis=0, tiled=True),
        w_gate[0],
        w_up[0],
        w_down[0],
    )
    expert_out = lax.psum_scatter(
        partial_out.astype(jnp.bfloat16), "tp", scatter_dimension=0, tiled=True
    )
    returned = lax.all_to_all(
        expert_out.reshape(expert_count, capacity, model_width),
        "sp",
        split_axis=0,
        concat_axis=0,
        tiled=True,
    )
    picked = returned.reshape(slot_total, model_width)[targets.reshape(-1)].astype(jnp.float32)
    picked = picked.reshape(route_rows, top_count, model_width)
    own_weights = lax.dynamic_slice_in_dim(route_weights, tp_here * route_rows, route_rows, 0)
    routed = jnp.sum(picked * own_weights[:, :, None], axis=1)
    return (own_rows.astype(jnp.float32) + routed).astype(jnp.bfloat16)


def solution(mesh):
    return jax.shard_map(
        local,
        mesh=mesh,
        in_specs=(
            P("sp", "tp"),
            P("sp", "tp"),
            P("sp"),
            P(None, "tp"),
            P("tp", None, None),
            P("tp", None, None),
            P("tp"),
            P("tp"),
            P("tp", None),
            P("sp", None),
            P(),
            P("sp", None),
            P("sp", None),
            P("sp", None, "tp"),
            P("sp", None, "tp"),
            P("sp", "tp", None),
        ),
        out_specs=P(("sp", "tp"), None),
        check_vma=False,
    )
```

profile of v0, /device:TPU:1, one launch (start us, length us, event | category | flops | bytes accessed | tf_op | source)
XLA Modules:
  0.0 238.0 jit_solution(8923473398704581098)
XLA Ops:
  6.5 0.9 slice_add_fusion.4
  7.4 3.9 %collective-permute-start = (s32[3]{0:T(128)S(1)}, s32[3]{0:T(128)S(1)}, u32[]{:S(2)}, u32[]{:S(2)}) collective-permute-start(s32[3]{0:T(128)S(1)} %slice_add_fusion.4), channel_id=1, source_target_pairs={{0,16},{16,32},{32,48},{48,64},{64,80},{80,96},{96,112},{112,128},... | collective-permute-start | bytes 44 | tf_op jit(solution)/shard_map/ppermute | solution.py:16
  11.3 0.7 slice.329
  12.0 3.1 %collective-permute-start.1 = (bf16[3,128]{1,0:T(4,128)(2,1)S(1)}, bf16[3,128]{1,0:T(4,128)(2,1)S(1)}, u32[]{:S(2)}, u32[]{:S(2)}) collective-permute-start(bf16[3,128]{1,0:T(4,128)(2,1)S(1)} %slice.329), channel_id=1, source_target_pairs={{0,16},{16,32},{32,48},{48,64},{64,80},{80,96},{96,112},{112,128},... | collective-permute-start | bytes 2312 | tf_op jit(solution)/shard_map/ppermute | solution.py:16
  15.1 0.8 bitcast_convert_fusion.3
  16.0 0.7 fusion.49
  16.6 0.0 collective-permute-done
  16.7 0.8 pad_add_fusion
  17.4 0.8 slice_compare_fusion
  18.2 0.0 collective-permute-done.1
  18.2 1.2 add_convert_fusion.1
  19.3 1.0 exponential_select_fusion
  20.3 0.9 fusion.15
  21.3 0.0 copy-start.2
  22.8 0.0 slice-start
  22.9 0.0 copy-start.1
  23.0 0.0 copy-start.3
  23.0 0.0 copy-start.5
  23.2 0.2 slice-done
  23.5 0.6 broadcast_in_dim.71
  24.1 6.2 %all-to-all-start = ((f32[16,2,128]{2,1,0:T(2,128)}), f32[16,2,128]{2,1,0:T(2,128)S(1)}, u32[]{:S(2)}, u32[]{:S(2)}) async-start(f32[16,2,128]{2,1,0:T(2,128)} %broadcast_in_dim.71), calls=%async_computation | async-start | bytes 32768 | tf_op jit(solution)/shard_map/all_to_all | solution.py:21
  30.3 6.4 %all-to-all-done = f32[16,2,128]{2,1,0:T(2,128)S(1)} async-done(((f32[16,2,128]{2,1,0:T(2,128)}), f32[16,2,128]{2,1,0:T(2,128)S(1)}, u32[]{:S(2)}, u32[]{:S(2)}) %all-to-all-start) | async-done | bytes 16416 | tf_op jit(solution)/shard_map/all_to_all | solution.py:21
  36.8 0.1 broadcast_select_fusion.1
  37.1 0.1 multiply_reduce_fusion.1
  37.2 18.3 %all_to_all.26 = f32[16,1,256]{2,1,0:T(1,128)S(1)} all-to-all(f32[16,1,256]{2,1,0:T(1,128)S(1)} %broadcast_in_dim.74), channel_id=1, replica_groups=mesh['sp'=16,'tp'=16] {'tp'}, dimensions={0} | all-to-all | bytes 32768 | tf_op jit(solution)/shard_map/all_to_all | solution.py:21
  55.6 0.0 copy-start.6
  55.6 1.5 convolution_convert_fusion.1
  57.1 4.0 %all-to-all-start.2 = ((bf16[16,16,2048]{2,1,0:T(8,128)(2,1)}), bf16[16,16,2048]{2,1,0:T(8,128)(2,1)S(1)}, u32[]{:S(2)}, u32[]{:S(2)}) async-start(bf16[16,16,2048]{2,1,0:T(8,128)(2,1)} %bitcast.9), calls=%async_computation.2 | async-start | bytes 2097152 | tf_op jit(solution)/shard_map/all_to_all | solution.py:75
  61.0 0.0 all-gather.2.cloned.1.call-start
  61.1 0.1 constant_dynamic-slice_fusion.1
  61.2 0.1 copy.35
  61.3 0.1 eq.40
  61.3 0.1 fusion.46
  61.4 0.1 reduce_window_sum.11
  61.5 0.2 select_reduce_fusion
  61.7 0.1 reduce_sum.71
  61.8 0.1 copy.31
  61.8 0.1 convert_reduce_fusion.1
  61.9 27.2 %all-to-all-done.2 = bf16[16,16,2048]{2,1,0:T(8,128)(2,1)S(1)} async-done(((bf16[16,16,2048]{2,1,0:T(8,128)(2,1)}), bf16[16,16,2048]{2,1,0:T(8,128)(2,1)S(1)}, u32[]{:S(2)}, u32[]{:S(2)}) %all-to-all-start.2) | async-done | bytes 1048608 | tf_op jit(solution)/shard_map/all_to_all | solution.py:75
  89.1 0.1 convert_reduce_fusion
  89.2 1.0 fusion.18
  90.2 0.3 convolution_convert_fusion.2
  90.5 0.1 reshape.120
  90.6 11.1 %all_to_all.27 = bf16[16,4,2048]{2,1,0:T(4,128)(2,1)S(1)} all-to-all(bf16[16,4,2048]{2,1,0:T(4,128)(2,1)S(1)} %reshape.120), channel_id=1, replica_groups=mesh['sp'=16,'tp'=16] {'sp'}, dimensions={0} | all-to-all | bytes 524288 | tf_op jit(solution)/shard_map/all_to_all | solution.py:202
  101.7 0.8 reshape.121
  102.5 0.0 all-gather.2.cloned.1.call-update
  102.5 0.0 reduce-scatter.2.cloned.1.call-start
  102.5 36.6 %all-gather.2.cloned.1.call-done = bf16[1024,2048]{1,0:T(8,128)(2,1)} async-done(((bf16[64,2048]{1,0:T(8,128)(2,1)}), bf16[1024,2048]{1,0:T(8,128)(2,1)}) %all-gather.2.cloned.1.call-update) | async-done | bytes 4194320 | tf_op jit(solution)/shard_map/all_gather | solution.py:210
  139.1 6.2 %fusion.3 = f32[1024,384]{1,0:T(8,128)} fusion(bf16[1024,2048]{1,0:T(8,128)(2,1)} %all-gather.2.cloned.1.call-done, bf16[1,2048,384]{2,1,0:T(8,128)(2,1)} %param.29), kind=kOutput, calls=%fused_computation.8 | convolution fusion | flops 1610612736 | bytes 7340032 | tf_op jit(solution)/shard_map/dot_general | solution.py:105
  145.3 9.6 %convolution_convert_fusion = bf16[1024,2048]{1,0:T(8,128)(2,1)} fusion(bf16[1,384,2048]{2,1,0:T(8,128)(2,1)S(1)} %copy-done, f32[1024,384]{1,0:T(8,128)} %fusion.3, bf16[1024,2048]{1,0:T(8,128)(2,1)} %all-gather.2.cloned.1.call-done, bf16[1,2048,384]{2,1,0:T(8,128)(2,1)} %param.30), kind=kOutput, calls=%fused_computation.1 | convolution fusion | flops 3225681920 | bytes 13107200 | tf_op jit(solution)/shard_map/dot_general | solution.py:108
  154.9 0.0 reduce-scatter.2.cloned.1.call-update
  155.0 0.1 mul.420
  155.0 0.6 copy-done.7
  155.6 0.1 constant_dynamic-slice_fusion
  155.7 0.1 copy.32
  155.8 57.7 %reduce-scatter.2.cloned.1.call-done = bf16[64,2048]{1,0:T(8,128)(2,1)} async-done(((bf16[1024,2048]{1,0:T(8,128)(2,1)}), bf16[64,2048]{1,0:T(8,128)(2,1)}) %reduce-scatter.2.cloned.1.call-update) | async-done | bytes 262160 | tf_op jit(solution)/shard_map/reduce_scatter | solution.py:215
  213.5 1.8 reshape.122
  215.2 6.4 %all-to-all-start.4 = ((bf16[16,4,2048]{2,1,0:T(4,128)(2,1)}), bf16[16,4,2048]{2,1,0:T(4,128)(2,1)S(1)}, u32[]{:S(2)}, u32[]{:S(2)}) async-start(bf16[16,4,2048]{2,1,0:T(4,128)(2,1)} %reshape.122), calls=%async_computation.5 | async-start | bytes 524288 | tf_op jit(solution)/shard_map/all_to_all | solution.py:218
  221.7 7.5 %all-to-all-done.4 = bf16[16,4,2048]{2,1,0:T(4,128)(2,1)S(1)} async-done(((bf16[16,4,2048]{2,1,0:T(4,128)(2,1)}), bf16[16,4,2048]{2,1,0:T(4,128)(2,1)S(1)}, u32[]{:S(2)}, u32[]{:S(2)}) %all-to-all-start.4) | async-done | bytes 262176 | tf_op jit(solution)/shard_map/all_to_all | solution.py:218
  229.2 0.1 reshape.123
  229.3 0.7 gather_fusion
  229.9 0.2 reshape.128
  230.1 0.4 multiply_reduce_fusion
  230.5 0.6 fusion.21
  (160 shorter events, 1.7 us)
Async XLA Ops:
  6.5 138.8 %copy-start = (bf16[1,384,2048]{2,1,0:T(8,128)(2,1)S(1)}, bf16[1,384,2048]{2,1,0:T(8,128)(2,1)}, u32[]{:S(2)}) copy-start(bf16[1,384,2048]{2,1,0:T(8,128)(2,1)} %param.31) | copy-start | bytes 4718596
  7.4 9.2 %collective-permute-start = (s32[3]{0:T(128)S(1)}, s32[3]{0:T(128)S(1)}, u32[]{:S(2)}, u32[]{:S(2)}) collective-permute-start(s32[3]{0:T(128)S(1)} %slice_add_fusion.4), channel_id=1, source_target_pairs={{0,16},{16,32},{32,48},{48,64},{64,80},{80,96},{96,112},{112,128},... | collective-permute-start | bytes 44 | tf_op jit(solution)/shard_map/ppermute | solution.py:16
  12.0 6.1 %collective-permute-start.1 = (bf16[3,128]{1,0:T(4,128)(2,1)S(1)}, bf16[3,128]{1,0:T(4,128)(2,1)S(1)}, u32[]{:S(2)}, u32[]{:S(2)}) collective-permute-start(bf16[3,128]{1,0:T(4,128)(2,1)S(1)} %slice.329), channel_id=1, source_target_pairs={{0,16},{16,32},{32,48},{48,64},{64,80},{80,96},{96,112},{112,128},... | collective-permute-start | bytes 2312 | tf_op jit(solution)/shard_map/ppermute | solution.py:16
  21.3 1.5 copy-start.2
  22.8 0.6 slice-start
  22.9 32.6 %copy-start.1 = (bf16[128,2048]{1,0:T(8,128)(2,1)S(1)}, bf16[128,2048]{1,0:T(8,128)(2,1)}, u32[]{:S(2)}) copy-start(bf16[128,2048]{1,0:T(8,128)(2,1)} %param.24) | copy-start | bytes 1572868
  23.0 32.6 %copy-start.3 = (bf16[256,128]{1,0:T(8,128)(2,1)S(1)}, bf16[256,128]{1,0:T(8,128)(2,1)}, u32[]{:S(2)}) copy-start(bf16[256,128]{1,0:T(8,128)(2,1)} %param.17) | copy-start | bytes 196612
  23.0 32.6 %copy-start.5 = (f32[128]{0:T(128)S(1)}, f32[128]{0:T(128)}, u32[]{:S(2)}) copy-start(f32[128]{0:T(128)} %param.23) | copy-start | bytes 1540
  24.1 12.6 %all-to-all-start = ((f32[16,2,128]{2,1,0:T(2,128)}), f32[16,2,128]{2,1,0:T(2,128)S(1)}, u32[]{:S(2)}, u32[]{:S(2)}) async-start(f32[16,2,128]{2,1,0:T(2,128)} %broadcast_in_dim.71), calls=%async_computation | async-start | bytes 32768 | tf_op jit(solution)/shard_map/all_to_all | solution.py:21
  55.6 5.5 %copy-start.6 = (s32[256,2]{0,1:T(2,128)S(1)}, s32[256,2]{0,1:T(2,128)}, u32[]{:S(2)}) copy-start(s32[256,2]{0,1:T(2,128)} %param.27) | copy-start | bytes 6148
  57.1 33.2 %copy-start.4 = (f32[2048]{0:T(1024)S(1)}, f32[2048]{0:T(1024)}, u32[]{:S(2)}) copy-start(f32[2048]{0:T(1024)} %param.26) | copy-start | bytes 24580
  57.1 32.0 %all-to-all-start.2 = ((bf16[16,16,2048]{2,1,0:T(8,128)(2,1)}), bf16[16,16,2048]{2,1,0:T(8,128)(2,1)S(1)}, u32[]{:S(2)}, u32[]{:S(2)}) async-start(bf16[16,16,2048]{2,1,0:T(8,128)(2,1)} %bitcast.9), calls=%async_computation.2 | async-start | bytes 2097152 | tf_op jit(solution)/shard_map/all_to_all | solution.py:75
  61.0 78.1 %all-gather.2.cloned.1.call-start = ((), (), s32[]{:S(2)}) async-start(), calls=%async_computation.6 | async-start | bytes 4456448 | tf_op jit(solution)/shard_map/all_gather | solution.py:210
  102.5 111.0 %reduce-scatter.2.cloned.1.call-start = ((), (), s32[]{:S(2)}) async-start(), calls=%async_computation.7 | async-start | bytes 4456448 | tf_op jit(solution)/shard_map/reduce_scatter | solution.py:215
  154.9 0.7 copy-start.7
  215.2 14.0 %all-to-all-start.4 = ((bf16[16,4,2048]{2,1,0:T(4,128)(2,1)}), bf16[16,4,2048]{2,1,0:T(4,128)(2,1)S(1)}, u32[]{:S(2)}, u32[]{:S(2)}) async-start(bf16[16,4,2048]{2,1,0:T(4,128)(2,1)} %reshape.122), calls=%async_computation.5 | async-start | bytes 524288 | tf_op jit(solution)/shard_map/all_to_all | solution.py:218
Sparse Core Ops, SparseCore 0:
  102.6 36.4 all-gather.1
  155.1 58.3 reduce-scatter.1
where the time goes:
time: 242 us; the launch traced here: 238 us
  waiting for transfers between devices  135 us (56%)
  blocking collectives  29.3 us (12%)
  starting transfers between devices  23.7 us (10%)
  matrix products  19.5 us (8%)
  between operations  14.3 us (6%)
  other arithmetic  8.28 us (3%)
  local copies, waits for them, and re-layouts  7.47 us (3%)
    reduce_scatter x1, waiting for transfers between devices, local(): lax.psum_scatter(partial_out.astype(jnp.bfloat16), 'tp', scatter_dimensio...  57.7 us
    all_gather x1, waiting for transfers between devices, local(): lax.all_gather(arrived.reshape(slot_total, model_width), 'tp', axis=0, ti...  36.6 us
    all_to_all x1, waiting for transfers between devices, summed_on_arrival(): lax.all_to_all(parts, axis, split_axis=0, concat_axis=0, tiled=True)  27.2 us
    all_to_all x1, blocking collectives, sent_to_all(): lax.all_to_all(jnp.broadcast_to(x[None], (devices, *x.shape)), axis, 0, 0...  18.3 us
    all_to_all x1, blocking collectives, local(): lax.all_to_all(outgoing.reshape(expert_count, capacity, model_width), 'sp...  11.1 us
    dot_general x1, matrix products, expert_apply(): jnp.dot(hidden_units, down_weight, preferred_element_type=jnp.float32)  9.62 us
    all_to_all x1, waiting for transfers between devices, local(): lax.all_to_all(expert_out.reshape(expert_count, capacity, model_width), '...  7.52 us
    ppermute x2, starting transfers between devices, shifted(): return lax.ppermute(block, axis, route)  7.03 us
  transfers between devices with their start and end apart: 7, of which 5 were waited for; matrix products, arithmetic and copies ran while one was open for 2% of the time, Pallas kernels for 0%

commit v1 on v0

v1 whole, which is shorter than its diff:
```python
import functools

import jax
import jax.numpy as jnp
from jax import lax
from jax.experimental import pallas as pl
from jax.experimental.pallas import tpu as pltpu
from jax.sharding import PartitionSpec as P

MESH = pl.DeviceIdType.MESH
F32 = jnp.float32
BF16 = jnp.bfloat16
EPSILON = 1e-06
RATE_SCALE = 8.0
PARTS = 4
LANES = 128
REACH = 3
ROUTE_ROWS = 16


def softplus_of_minus(v):
    t = jnp.exp(-jnp.abs(v))
    s = t / (2.0 + t)
    s2 = s * s
    total = jnp.full_like(s, 1.0 / 19.0)
    for odd in (17, 15, 13, 11, 9, 7, 5, 3, 1):
        total = total * s2 + 1.0 / odd
    return jnp.maximum(-v, 0.0) + 2.0 * s * total


def one_minus_exp_of_minus(y, exp_minus_y):
    total = jnp.ones_like(y)
    for n in (8, 7, 6, 5, 4, 3, 2):
        total = 1.0 - y * (1.0 / n) * total
    return jnp.where(y < 0.5, y * total, 1.0 - exp_minus_y)


def gelu(v):
    return 0.5 * v * (1.0 + jnp.tanh(0.7978845608028654 * (v + 0.044715 * v * v * v)))


def iota(shape, dim):
    return lax.broadcasted_iota(jnp.int32, shape, dim)


def column_of(row, first, count):
    shape = (count, row.shape[1])
    return jnp.sum(
        jnp.where(iota(shape, 1) == iota(shape, 0) + first, row, 0.0), axis=1, keepdims=True
    )


def row_of(column, width):
    shape = (column.shape[0], width)
    return jnp.sum(jnp.where(iota(shape, 1) == iota(shape, 0), column, 0.0), axis=0, keepdims=True)


def kernel(
    n_sp,
    n_tp,
    lru,
    gate,
    docs,
    taps,
    rate,
    inlet,
    decay,
    gain,
    fgain,
    routes,
    rweights,
    w_out_hbm,
    resid_hbm,
    wg_hbm,
    wu_hbm,
    wd_hbm,
    out,
    xs,
    ds,
    a_s,
    b_s,
    hs,
    rx,
    cs,
    hd,
    w_out,
    resid,
    wg,
    wu,
    wd,
    sqb,
    sq2,
    pp,
    psib,
    pst,
    prp,
    prm,
    og,
    xg,
    po,
    sib,
    st,
    rp,
    rm,
    ret,
    rt,
    fo,
    fin,
    load_sem,
    fr_send,
    fr_recv,
    sq_send,
    sq_recv,
    s2_send,
    s2_recv,
    psib_send,
    psib_recv,
    prp_send,
    prp_recv,
    prm_send,
    prm_recv,
    di_send,
    di_recv,
    agp_send,
    agp_recv,
    agm_send,
    agm_recv,
    ags_send,
    ags_recv,
    sib_send,
    sib_recv,
    rp_send,
    rp_recv,
    rm_send,
    rm_recv,
    ret_send,
    ret_recv,
    fin_send,
    fin_recv,
):
    positions = lru.shape[0]
    model = wg.shape[0]
    width = model // PARTS
    n_z = n_tp // 2
    hops = n_z // 2
    quads = n_tp // PARTS
    tokens = positions // quads
    slot_rows = rt.shape[1]
    cap = slot_rows // PARTS
    half_slots = n_sp * slot_rows // 2
    half_tokens = tokens // 2
    s_me = lax.axis_index("sp")
    t_me = lax.axis_index("tp")
    z_me = lax.div(t_me, 2)
    c_me = lax.rem(t_me, 2)
    q_me = lax.div(t_me, PARTS)
    p_me = lax.rem(t_me, PARTS)
    sibling = z_me * 2 + (1 - c_me)
    up = lax.rem(z_me + 1, n_z) * 2 + c_me
    down = lax.rem(z_me + n_z - 1, n_z) * 2 + c_me

    def sp_peer(d):
        return lax.rem(s_me + d, n_sp)

    def tp_peer(d):
        return lax.rem(t_me + d, n_tp)

    def remote(src, dst, send, recv, **where):
        return pltpu.make_async_remote_copy(
            src_ref=src,
            dst_ref=dst,
            send_sem=send,
            recv_sem=recv,
            device_id=where,
            device_id_type=MESH,
        )

    def cols(part):
        return pl.ds(pl.multiple_of(part * width, LANES), width)

    def rows(start, size):
        return pl.ds(pl.multiple_of(start, 8), size)

    barrier = pltpu.get_barrier_semaphore()
    for d in range(1, n_sp):
        pl.semaphore_signal(barrier, inc=1, device_id={"sp": sp_peer(d)}, device_id_type=MESH)
    for d in range(1, n_tp):
        pl.semaphore_signal(barrier, inc=1, device_id={"tp": tp_peer(d)}, device_id_type=MESH)

    loads = [
        pltpu.make_async_copy(w_out_hbm, w_out, load_sem.at[0]),
        pltpu.make_async_copy(
            resid_hbm.at[rows(q_me * tokens, tokens), cols(p_me)], resid, load_sem.at[1]
        ),
        pltpu.make_async_copy(wg_hbm, wg, load_sem.at[2]),
        pltpu.make_async_copy(wu_hbm, wu, load_sem.at[3]),
        pltpu.make_async_copy(wd_hbm, wd, load_sem.at[4]),
    ]
    for load in loads:
        load.start()

    softplus = softplus_of_minus(decay[...])
    tap = [taps[k : k + 1, :].astype(F32) for k in range(REACH + 1)]

    def gates(convolved, starts):
        rate_gate = jax.nn.sigmoid(jnp.dot(convolved, rate[...], preferred_element_type=F32))
        inlet_gate = jax.nn.sigmoid(jnp.dot(convolved, inlet[...], preferred_element_type=F32))
        log_decay = -RATE_SCALE * rate_gate * softplus
        step = jnp.exp(log_decay)
        norm = jnp.sqrt(one_minus_exp_of_minus(-2.0 * log_decay, step * step))
        norm = jnp.where(starts, 1.0, norm)
        return jnp.where(starts, 0.0, step), norm * inlet_gate * convolved.astype(F32)

    doc_col = jnp.broadcast_to(
        column_of(docs[...].astype(F32), 0, positions), (positions, LANES)
    )
    x = lru[...].astype(F32)
    xs[0:8, :] = jnp.zeros((8, LANES), F32)
    xs[pl.ds(8, positions), :] = x
    ds[0:8, :] = jnp.full((8, LANES), -1.0, F32)
    ds[pl.ds(8, positions), :] = doc_col
    conv = jnp.zeros((positions, LANES), F32)
    for k in range(REACH + 1):
        back = 8 - REACH + k
        same = ds[pl.ds(back, positions), :] == doc_col
        conv = conv + jnp.where(same, xs[pl.ds(back, positions), :] * tap[k], 0.0)
    step, drive = gates(conv.astype(BF16), ds[pl.ds(7, positions), :] != doc_col)
    head = iota((positions, LANES), 0) < REACH
    step = jnp.where(head, 1.0, step)
    drive = jnp.where(head, 0.0, drive)
    run = positions // 8
    pitch = run + 8
    for j in range(8):
        a_s[pl.ds(j * pitch, run), :] = step[j * run : (j + 1) * run, :]
        b_s[pl.ds(j * pitch, run), :] = drive[j * run : (j + 1) * run, :]
    total_a = a_s[pl.ds(0, 8, stride=pitch), :]
    total_b = b_s[pl.ds(0, 8, stride=pitch), :]
    for i in range(1, run):
        here = a_s[pl.ds(i, 8, stride=pitch), :]
        total_b = here * total_b + b_s[pl.ds(i, 8, stride=pitch), :]
        total_a = here * total_a
        a_s[pl.ds(i, 8, stride=pitch), :] = total_a
        b_s[pl.ds(i, 8, stride=pitch), :] = total_b
    ahead_a = [jnp.ones((1, LANES), F32)]
    ahead_b = [jnp.zeros((1, LANES), F32)]
    for j in range(8):
        ahead_b.append(total_a[j : j + 1, :] * ahead_b[j] + total_b[j : j + 1, :])
        ahead_a.append(total_a[j : j + 1, :] * ahead_a[j])

    rx[0:16, :] = jnp.where(iota((16, LANES), 0) < 8, 0.0, jnp.full((16, LANES), -1.0, F32))
    own = pl.multiple_of((s_me + 1) * 16, 16)
    last = 8 + positions - REACH
    rx[pl.ds(own, 1), :] = ahead_a[8]
    rx[pl.ds(own + 1, 1), :] = ahead_b[8]
    rx[pl.ds(own + 2, REACH), :] = xs[8 : 8 + REACH, :]
    rx[pl.ds(own + 5, REACH), :] = xs[last : last + REACH, :]
    rx[pl.ds(own + 8, REACH), :] = ds[8 : 8 + REACH, :]
    rx[pl.ds(own + 11, REACH), :] = ds[last : last + REACH, :]
    rx[pl.ds(own + 14, 2), :] = jnp.zeros((2, LANES), F32)

    pl.semaphore_wait(barrier, n_sp + n_tp - 2)

    def front_copy(d, source):
        block = rx.at[rows((source + 1) * 16, 16), :]
        return remote(block, block, fr_send.at[d], fr_recv.at[source], sp=sp_peer(d))

    for d in range(1, n_sp):
        front_copy(d, s_me).start()
    gelu_gain = gelu(gate[...].astype(F32)) * gain[...]
    for d in range(1, n_sp):
        front_copy(d, sp_peer(d)).wait_recv()

    seq = [rx[pl.ds(5 + k, n_sp, stride=16), :] for k in range(REACH)]
    seq += [rx[pl.ds(18 + k, n_sp, stride=16), :] for k in range(REACH)]
    dseq = [rx[pl.ds(11 + k, n_sp, stride=16), :] for k in range(REACH)]
    dseq += [rx[pl.ds(24 + k, n_sp, stride=16), :] for k in range(REACH)]
    head_a, head_b = [], []
    for k in range(REACH):
        conv = jnp.zeros((n_sp, LANES), F32)
        for m in range(REACH + 1):
            conv = conv + jnp.where(dseq[k + m] == dseq[k + REACH], seq[k + m] * tap[m], 0.0)
        one_a, one_b = gates(conv.astype(BF16), dseq[k + REACH] != dseq[k + REACH - 1])
        head_a.append(one_a)
        head_b.append(one_b)
        hd[pl.ds(2 * k * n_sp, n_sp), :] = one_a
        hd[pl.ds((2 * k + 1) * n_sp, n_sp), :] = one_b
    body_a = rx[pl.ds(16, n_sp, stride=16), :]
    body_b = rx[pl.ds(17, n_sp, stride=16), :]
    all_b = (head_b[0] * head_a[1] + head_b[1]) * head_a[2] + head_b[2]
    cs[0:n_sp, :] = head_a[0] * head_a[1] * head_a[2] * body_a
    cs[n_sp : 2 * n_sp, :] = all_b * body_a + body_b
    state = jnp.zeros((1, LANES), F32)
    for s in range(n_sp - 1):
        state = jnp.where(s < s_me, cs[s : s + 1, :] * state + cs[n_sp + s : n_sp + s + 1, :], state)
    first = []
    for k in range(REACH):
        state = hd[pl.ds(2 * k * n_sp + s_me, 1), :] * state + hd[
            pl.ds((2 * k + 1) * n_sp + s_me, 1), :
        ]
        first.append(state)
    for j in range(8):
        carry = ahead_b[j] + ahead_a[j] * state
        piece = b_s[pl.ds(j * pitch, run), :] + a_s[pl.ds(j * pitch, run), :] * carry
        if j == 0:
            at = iota((run, LANES), 0)
            piece = jnp.where(at == 0, first[0], jnp.where(at == 1, first[1], piece))
        hs[pl.ds(j * run, run), :] = piece
    hidden = hs[...]

    sqb[pl.ds(t_me, 1), :, :] = row_of(
        jnp.sum(hidden * hidden, axis=1, keepdims=True), positions
    ).reshape(1, 1, positions)

    def square_copy(d, source):
        return remote(
            sqb.at[source], sqb.at[source], sq_send.at[d], sq_recv.at[source], tp=tp_peer(d)
        )

    mixer = (hidden * gelu_gain).astype(BF16)
    loads[0].wait()
    for part in range(PARTS):
        block = jnp.dot(
            mixer, w_out[:, part * width : (part + 1) * width], preferred_element_type=F32
        ).astype(BF16)
        for q in range(quads):
            pp[q, :, part * width : (part + 1) * width] = block[q * tokens : (q + 1) * tokens, :]
    for d in range(1, n_tp):
        square_copy(d, t_me).start()

    def to_sibling(src, dst, send, recv, q):
        copies = []
        for j in range(2):
            chip = 2 * q + j
            copies.append(
                remote(
                    src.at[q, :, cols(2 * j + 1 - c_me)],
                    dst.at[chip],
                    send.at[chip],
                    recv.at[chip],
                    tp=sibling,
                )
            )
        return copies

    def reduce_scatter(src, sib_buf, stage, buf_p, buf_m, sems, half):
        sib_s, sib_r, p_s, p_r, m_s, m_r = sems
        arrived = []

        def chip_at(offset):
            return lax.rem(z_me + offset + 2 * n_z, n_z)

        def wait_sibling(chip):
            remote(
                sib_buf.at[chip], sib_buf.at[chip], sib_s.at[chip], sib_r.at[chip], tp=sibling
            ).wait_recv()

        def term(chip, h):
            at = pl.ds(h * half, half)
            mine = src[lax.div(chip, 2), at, cols(lax.rem(chip, 2) * 2 + c_me)]
            return mine.astype(F32) + sib_buf[chip, at, :].astype(F32)

        def length(direction, h):
            return hops if (direction > 0) == (h == 0) else hops - 1

        def hop(direction, h, j, source):
            buf = buf_p if direction > 0 else buf_m
            sends, recvs = (p_s, p_r) if direction > 0 else (m_s, m_r)
            target = up if direction > 0 else down
            return remote(
                source, buf.at[h, j - 1], sends.at[h, j - 1], recvs.at[h, j - 1], tp=target
            )

        def arrival(direction, h, j):
            buf = buf_p if direction > 0 else buf_m
            return buf.at[h, j - 1]

        lanes = [(1, 0), (-1, 1), (1, 1), (-1, 0)]
        wait_sibling(chip_at(hops))
        for n, (direction, h) in enumerate(lanes):
            if n == 2:
                wait_sibling(chip_at(hops - 1))
                if hops > 1:
                    wait_sibling(chip_at(1 - hops))
            if length(direction, h) == 0:
                continue
            stage[n] = term(chip_at(direction * length(direction, h)), h).astype(BF16)
            hop(direction, h, 1, stage.at[n]).start()
        for d in range(hops - 2, -1, -1):
            wait_sibling(chip_at(d))
            if d > 0:
                wait_sibling(chip_at(-d))

        def step_of(j, _):
            for direction, h in lanes:
                n = length(direction, h)

                def one(direction=direction, h=h, n=n):
                    slot = arrival(direction, h, j - 1)
                    hop(direction, h, j - 1, slot).wait_recv()
                    value = term(chip_at(direction * (n + 1 - j)), h) + slot[...].astype(F32)
                    slot[...] = value.astype(BF16)
                    hop(direction, h, j, slot).start()

                if n == hops:
                    one()
                else:
                    pl.when(j < hops)(one)
            return 0

        lax.fori_loop(2, hops + 1, step_of, 0)
        for h in range(2):
            total = term(z_me, h)
            for direction in (1, -1):
                n = length(direction, h)
                if n:
                    slot = arrival(direction, h, n)
                    hop(direction, h, n, slot).wait_recv()
                    total = total + slot[...].astype(F32)
            arrived.append(total)
        for n, (direction, h) in enumerate(lanes):
            for j in range(1, length(direction, h) + 1):
                hop(direction, h, j, arrival(direction, h, j)).wait_send()
        return arrived

    copies = []
    for q in range(quads):
        copies += to_sibling(pp, psib, psib_send, psib_recv, q)
    for copy in copies:
        copy.start()
    parts = reduce_scatter(
        pp,
        psib,
        pst,
        prp,
        prm,
        (psib_send, psib_recv, prp_send, prp_recv, prm_send, prm_recv),
        half_tokens,
    )
    for copy in copies:
        copy.wait_send()
    for d in range(1, n_tp):
        square_copy(d, tp_peer(d)).wait_recv()
    squares = sqb[0]
    for t in range(1, n_tp):
        squares = squares + sqb[t]
    inverse = lax.rsqrt(squares / (n_tp * LANES) + EPSILON)
    inverse = column_of(inverse, q_me * tokens, tokens)
    loads[1].wait()
    for h in range(2):
        at = slice(h * half_tokens, (h + 1) * half_tokens)
        resid[at, :] = (
            resid[at, :].astype(F32) + parts[h] * inverse[at, :]
        ).astype(BF16)
    after = resid[...].astype(F32)
    sq2[pl.ds(p_me, 1), :, :] = row_of(
        jnp.sum(after * after, axis=1, keepdims=True), LANES
    ).reshape(1, 1, LANES)

    def quad_peer(d):
        return lax.rem(p_me + d, PARTS)

    def norm_copy(d, source):
        return remote(
            sq2.at[source],
            sq2.at[source],
            s2_send.at[d],
            s2_recv.at[source],
            tp=q_me * PARTS + quad_peer(d),
        )

    for d in range(1, PARTS):
        norm_copy(d, p_me).start()

    slots = n_sp * slot_rows
    shape = (tokens, slots)
    lane, token = iota(shape, 1), iota(shape, 0)
    expert = lax.div(lane, slot_rows)
    block = lax.div(lax.rem(lane, slot_rows), cap)
    place = lax.rem(lane, cap).astype(F32)
    here = block == lax.div(token, ROUTE_ROWS)
    expert = expert.astype(F32)
    route_rows = routes[...].astype(F32)
    named = [
        here & (column_of(route_rows[k : k + 1, :], q_me * tokens, tokens) == expert)
        for k in range(2)
    ]
    chosen = jnp.where(named[0] | named[1], 1.0, 0.0)
    earlier = jnp.where(iota((tokens, tokens), 1) < iota((tokens, tokens), 0), 1.0, 0.0)
    rank = jnp.dot(earlier.astype(BF16), chosen.astype(BF16), preferred_element_type=F32)
    pick = jnp.where(rank == place, chosen, 0.0)
    weight = jnp.zeros(shape, F32)
    for k in range(2):
        own_weight = column_of(rweights[k : k + 1, :], q_me * tokens, tokens)
        weight = weight + jnp.where(named[k], own_weight * pick, 0.0)
    weight_high = weight.astype(BF16)
    weight_low = (weight - weight_high.astype(F32)).astype(BF16)
    scale = fgain[:, cols(p_me)]
    for d in range(1, PARTS):
        norm_copy(d, quad_peer(d)).wait_recv()
    squares = sq2[0] + sq2[1] + sq2[2] + sq2[3]
    inverse = column_of(lax.rsqrt(squares / model + EPSILON), 0, tokens)
    normed = (after * inverse * scale).astype(BF16)
    outgoing = lax.dot_general(
        pick.astype(BF16), normed, (((0,), (0,)), ((), ())), preferred_element_type=F32
    ).astype(BF16)
    og[...] = outgoing.reshape(n_sp, slot_rows, width)
    xg[q_me, rows(s_me * slot_rows, slot_rows), cols(p_me)] = og[s_me]

    def dispatch_copy(d, source, peer):
        return remote(
            og.at[peer],
            xg.at[q_me, rows(source * slot_rows, slot_rows), cols(p_me)],
            di_send.at[d],
            di_recv.at[source],
            sp=peer,
        )

    for d in range(1, n_sp):
        dispatch_copy(d, s_me, sp_peer(d)).start()

    def sub_block(chip, h, core):
        return xg.at[
            lax.div(chip, 2),
            pl.ds(h * half_slots, half_slots),
            cols(lax.rem(chip, 2) * 2 + core),
        ]

    def ring_copy(direction, h, k, chip):
        sends, recvs = (agp_send, agp_recv) if direction > 0 else (agm_send, agm_recv)
        view = sub_block(chip, h, c_me)
        return remote(
            view, view, sends.at[h, k], recvs.at[h, k], tp=up if direction > 0 else down
        )

    def across_copy(h, chip, core):
        view = sub_block(chip, h, core)
        return remote(view, view, ags_send.at[h, chip], ags_recv.at[h, chip], tp=sibling)

    def reach(direction, h):
        return hops if (direction > 0) == (h == 0) else hops - 1

    for h in range(2):
        for source in range(h * n_sp // 2, (h + 1) * n_sp // 2):
            @pl.when(source != s_me)
            def _(source=source):
                remote(
                    og.at[source],
                    xg.at[q_me, rows(source * slot_rows, slot_rows), cols(p_me)],
                    di_send.at[0],
                    di_recv.at[source],
                    sp=sp_peer(1),
                ).wait_recv()
        for direction in (1, -1):
            if reach(direction, h):
                ring_copy(direction, h, 0, z_me).start()
        across_copy(h, z_me, c_me).start()
    for load in loads[2:]:
        load.wait()
    turn = 2 * lax.rem(z_me, 2) - 1

    def gather_step(k, _):
        for direction, h in ((1, 0), (-1, 1), (1, 1), (-1, 0)):
            n = reach(direction, h)

            def arrive(direction=direction, h=h, n=n):
                chip = lax.rem(z_me - direction * k + 2 * n_z, n_z)
                ring_copy(direction, h, k - 1, chip).wait_recv()

                @pl.when(k < n)
                def _():
                    ring_copy(direction, h, k, chip).start()

                across_copy(h, chip, c_me).start()

            if n == hops:
                arrive()
            else:
                pl.when(k < hops)(arrive)
        far = lax.div(k, 2)
        offset = jnp.where(lax.rem(k, 2) == 0, turn * far, -turn * far)
        q = lax.rem(q_me + offset + 2 * quads, quads)
        for j in range(2):
            for h in range(2):
                across_copy(h, 2 * q + j, 1 - c_me).wait_recv()
        rows_in = xg[q]
        gate_part = jnp.dot(rows_in, wg[...], preferred_element_type=F32)
        up_part = jnp.dot(rows_in, wu[...], preferred_element_type=F32)
        units = (jax.nn.silu(gate_part) * up_part).astype(BF16)
        for part in range(PARTS):
            at = slice(part * width, (part + 1) * width)
            po[q, :, at] = jnp.dot(units, wd[:, at], preferred_element_type=F32).astype(BF16)
        for copy in to_sibling(po, sib, sib_send, sib_recv, q):
            copy.start()
        return 0

    lax.fori_loop(1, hops + 1, gather_step, 0)

    parts = reduce_scatter(
        po,
        sib,
        st,
        rp,
        rm,
        (sib_send, sib_recv, rp_send, rp_recv, rm_send, rm_recv),
        half_slots,
    )
    half_sp = n_sp // 2
    for h in range(2):
        ret[h * half_sp : (h + 1) * half_sp] = (
            parts[h].astype(BF16).reshape(half_sp, slot_rows, width)
        )
    rt[pl.ds(s_me, 1)] = ret[pl.ds(s_me, 1)]

    def return_copy(d, source, peer):
        return remote(
            ret.at[peer], rt.at[source], ret_send.at[d], ret_recv.at[source], sp=peer
        )

    for d in range(1, n_sp):
        return_copy(d, s_me, sp_peer(d)).start()
    for d in range(1, n_sp):
        return_copy(d, sp_peer(d), sp_peer(d)).wait_recv()
    back = rt[...].reshape(slots, width)
    routed = jnp.dot(weight_high, back, preferred_element_type=F32) + jnp.dot(
        weight_low, back, preferred_element_type=F32
    )
    fo[...] = (resid[...].astype(F32) + routed).astype(BF16).reshape(PARTS, ROUTE_ROWS, width)
    fin[pl.ds(p_me, 1)] = fo[pl.ds(p_me, 1)]

    def final_copy(d, source, peer):
        return remote(
            fo.at[peer],
            fin.at[source],
            fin_send.at[d],
            fin_recv.at[source],
            tp=q_me * PARTS + peer,
        )

    for d in range(1, PARTS):
        final_copy(d, p_me, quad_peer(d)).start()
    for d in range(1, PARTS):
        final_copy(d, quad_peer(d), quad_peer(d)).wait_recv()
    for part in range(PARTS):
        out[:, part * width : (part + 1) * width] = fin[part]

    for d in range(1, n_sp):
        front_copy(d, s_me).wait_send()
        dispatch_copy(d, s_me, sp_peer(d)).wait_send()
        return_copy(d, s_me, sp_peer(d)).wait_send()
    for d in range(1, n_tp):
        square_copy(d, t_me).wait_send()
    for d in range(1, PARTS):
        norm_copy(d, p_me).wait_send()
        final_copy(d, p_me, quad_peer(d)).wait_send()
    for h in range(2):
        for direction in (1, -1):
            for k in range(reach(direction, h)):
                ring_copy(direction, h, k, z_me).wait_send()
        for chip in range(n_z):
            across_copy(h, chip, c_me).wait_send()
    for q in range(quads):
        for copy in to_sibling(po, sib, sib_send, sib_recv, q):
            copy.wait_send()


def local(
    n_sp,
    n_tp,
    lru_input,
    gate_input,
    documents,
    conv_taps,
    rate_weight,
    inlet_weight,
    decay_param,
    lru_gain,
    out_weight,
    residual,
    ffn_gain,
    routes,
    route_weights,
    w_gate,
    w_up,
    w_down,
):
    positions, channels = lru_input.shape
    model = residual.shape[1]
    units = w_gate.shape[2]
    width = model // PARTS
    n_z = n_tp // 2
    hops = n_z // 2
    quads = n_tp // PARTS
    tokens = positions // quads
    cap = 2 * routes.shape[1] * ROUTE_ROWS // n_sp
    slot_rows = PARTS * cap
    block_rows = n_sp * slot_rows
    pitch = positions + 64
    vmem = pl.BlockSpec(memory_space=pltpu.VMEM)
    hbm = pl.BlockSpec(memory_space=pl.ANY)
    dma = pltpu.SemaphoreType.DMA
    scratch = [
        pltpu.VMEM((positions + 8, LANES), F32),
        pltpu.VMEM((positions + 8, LANES), F32),
        pltpu.VMEM((pitch, LANES), F32),
        pltpu.VMEM((pitch, LANES), F32),
        pltpu.VMEM((positions, LANES), F32),
        pltpu.VMEM(((n_sp + 1) * 16, LANES), F32),
        pltpu.VMEM((2 * n_sp, LANES), F32),
        pltpu.VMEM((6 * n_sp, LANES), F32),
        pltpu.VMEM((channels, model), BF16),
        pltpu.VMEM((tokens, width), BF16),
        pltpu.VMEM((model, units), BF16),
        pltpu.VMEM((model, units), BF16),
        pltpu.VMEM((units, model), BF16),
        pltpu.VMEM((n_tp, 1, positions), F32),
        pltpu.VMEM((PARTS, 1, LANES), F32),
        pltpu.VMEM((quads, tokens, model), BF16),
        pltpu.VMEM((n_z, tokens, width), BF16),
        pltpu.VMEM((4, tokens // 2, width), BF16),
        pltpu.VMEM((2, hops, tokens // 2, width), BF16),
        pltpu.VMEM((2, hops, tokens // 2, width), BF16),
        pltpu.VMEM((n_sp, slot_rows, width), BF16),
        pltpu.VMEM((quads, block_rows, model), BF16),
        pltpu.VMEM((quads, block_rows, model), BF16),
        pltpu.VMEM((n_z, block_rows, width), BF16),
        pltpu.VMEM((4, block_rows // 2, width), BF16),
        pltpu.VMEM((2, hops, block_rows // 2, width), BF16),
        pltpu.VMEM((2, hops, block_rows // 2, width), BF16),
        pltpu.VMEM((n_sp, slot_rows, width), BF16),
        pltpu.VMEM((n_sp, slot_rows, width), BF16),
        pltpu.VMEM((PARTS, ROUTE_ROWS, width), BF16),
        pltpu.VMEM((PARTS, ROUTE_ROWS, width), BF16),
        dma((5,)),
        dma((n_sp,)),
        dma((n_sp,)),
        dma((n_tp,)),
        dma((n_tp,)),
        dma((PARTS,)),
        dma((PARTS,)),
        dma((n_z,)),
        dma((n_z,)),
        dma((2, hops)),
        dma((2, hops)),
        dma((2, hops)),
        dma((2, hops)),
        dma((n_sp,)),
        dma((n_sp,)),
        dma((2, hops)),
        dma((2, hops)),
        dma((2, hops)),
        dma((2, hops)),
        dma((2, n_z)),
        dma((2, n_z)),
        dma((n_z,)),
        dma((n_z,)),
        dma((2, hops)),
        dma((2, hops)),
        dma((2, hops)),
        dma((2, hops)),
        dma((n_sp,)),
        dma((n_sp,)),
        dma((PARTS,)),
        dma((PARTS,)),
    ]
    return pl.pallas_call(
        functools.partial(kernel, n_sp, n_tp),
        out_shape=jax.ShapeDtypeStruct((positions // n_tp, model), BF16),
        in_specs=[vmem] * 11 + [hbm] * 5,
        out_specs=vmem,
        scratch_shapes=scratch,
        name="layer",
        compiler_params=pltpu.CompilerParams(
            collective_id=0, has_side_effects=True, vmem_limit_bytes=56 * 1024 * 1024
        ),
    )(
        lru_input,
        gate_input,
        documents.reshape(1, positions),
        conv_taps,
        rate_weight[0],
        inlet_weight[0],
        decay_param.reshape(1, channels),
        lru_gain.reshape(1, channels),
        ffn_gain.reshape(1, model),
        routes.T,
        route_weights.T,
        out_weight,
        residual,
        w_gate[0],
        w_up[0],
        w_down[0],
    )


def solution(mesh):
    return jax.shard_map(
        functools.partial(local, mesh.shape["sp"], mesh.shape["tp"]),
        mesh=mesh,
        in_specs=(
            P("sp", "tp"),
            P("sp", "tp"),
            P("sp"),
            P(None, "tp"),
            P("tp", None, None),
            P("tp", None, None),
            P("tp"),
            P("tp"),
            P("tp", None),
            P("sp", None),
            P(),
            P("sp", None),
            P("sp", None),
            P("sp", None, "tp"),
            P("sp", None, "tp"),
            P("sp", "tp", None),
        ),
        out_specs=P(("sp", "tp"), None),
        check_vma=False,
    )
```

time: 242 us -> 104 us (0.43); the launches traced: 238 us -> 104 us
  waiting for transfers between devices: 135 us -> 0 us
  Pallas kernels: 0 us -> 103 us
  blocking collectives: 29.3 us -> 0 us
  starting transfers between devices: 23.7 us -> 0 us
  matrix products: 19.5 us -> 0 us
  between operations: 14.3 us -> 0.01 us
  other arithmetic: 8.28 us -> 0 us
  local copies, waits for them, and re-layouts: 7.47 us -> 1.47 us
    pallas_call x0 -> x1, Pallas kernels: none -> 103 us  [local(): pl.pallas_call(functools.partial(kernel, n_sp, n_tp), out_shape=jax.Shape...]
    reduce_scatter x1 -> x0, waiting for transfers between devices: 57.7 us -> none  [local(): lax.psum_scatter(partial_out.astype(jnp.bfloat16), 'tp', scatter_dimensio...]
    all_to_all x3 -> x0, waiting for transfers between devices: 41.1 us -> none  [the longest x1 27.2 us: summed_on_arrival(): lax.all_to_all(parts, axis, split_axis=0, concat_axis=0, tiled=True)]
    all_gather x1 -> x0, waiting for transfers between devices: 36.6 us -> none  [local(): lax.all_gather(arrived.reshape(slot_total, model_width), 'tp', axis=0, ti...]
    all_to_all x2 -> x0, blocking collectives: 29.3 us -> none  [the longest x1 18.3 us: sent_to_all(): lax.all_to_all(jnp.broadcast_to(x[None], (devices, *x.shape)), axis, 0, 0...]
    dot_general x6 -> x0, matrix products: 19.5 us -> none  [the longest x1 9.62 us: expert_apply(): jnp.dot(hidden_units, down_weight, preferred_element_type=jnp.float32)]
    all_to_all x3 -> x0, starting transfers between devices: 16.6 us -> none  [the longest x1 6.42 us: local(): lax.all_to_all(expert_out.reshape(expert_count, capacity, model_width), '...]
    ppermute x2 -> x0, starting transfers between devices: 7.03 us -> none  [shifted(): return lax.ppermute(block, axis, route)]
  transfers between devices with their start and end apart: 7 -> 0, of which waited for: 5 -> 0; matrix products, arithmetic and copies ran while one was open for 2% -> 0% of each run, Pallas kernels for 0% -> 0%
where the time goes in v1:
time: 104 us
  Pallas kernels  103 us (99%)
  local copies, waits for them, and re-layouts  1.47 us (1%)
    pallas_call x1, Pallas kernels, local(): pl.pallas_call(functools.partial(kernel, n_sp, n_tp), out_shape=jax.Shape...  103 us

profile of v1, /device:TPU:1, one launch (start us, length us, event | category | flops | bytes accessed | tf_op | source)
XLA Modules:
  0.0 104.2 jit_solution(12297515582153924209)
XLA Ops:
  0.0 102.7 %layer.1 = bf16[16,2048]{1,0:T(8,128)(2,1)} custom-call(bf16[256,128]{1,0:T(8,128)(2,1)} %lru.1, bf16[256,128]{1,0:T(8,128)(2,1)} %gate.1, s32[1,256]{1,0:T(1,128)} %bitcast.19, bf16[4,128]{1,0:T(4,128)(2,1)} %taps.1, bf16[128,128]{1,0:T(8,128)(2,1)} %bitcast.14, bf16[128,128]{1,0:T(8,128)(2,1)} %bitcast.15, f32[1,128]{1,0:T(1,128)} %bitcast.20, ...), custom_call_target="tpu_custom_call" | custom-call | tf_op jit(solution)/shard_map/layer/pallas_call | solution.py:765
  102.7 1.5 %copy.18 = bf16[16,2048]{1,0:T(8,128)(2,1)} copy(bf16[16,2048]{1,0:T(8,128)(2,1)} %layer.1) | data formatting | bytes 131072

commit v2 on v1

--- a/solution.py
+++ b/solution.py
@@ -41,6 +41,14 @@
 
 def iota(shape, dim):
     return lax.broadcasted_iota(jnp.int32, shape, dim)
+
+
+def when(condition, body):
+    if isinstance(condition, bool):
+        if condition:
+            body()
+    else:
+        pl.when(condition)(body)
 
 
 def column_of(row, first, count):
@@ -95,10 +103,23 @@
     pst,
     prp,
     prm,
+    pk,
+    wh,
+    wl,
     og,
+    xa,
+    ox,
     xg,
     po,
     sib,
+    xsib,
+    xo,
+    xi,
+    co,
+    hs_out,
+    hp,
+    hm,
+    gs,
     st,
     rp,
     rm,
@@ -127,8 +148,24 @@
     agm_recv,
     ags_send,
     ags_recv,
+    xap_send,
+    xap_recv,
+    xam_send,
+    xam_recv,
+    ox_send,
+    ox_recv,
+    xf_send,
+    xf_recv,
     sib_send,
     sib_recv,
+    xsib_send,
+    xsib_recv,
+    xo_send,
+    xo_recv,
+    hp_send,
+    hp_recv,
+    hm_send,
+    hm_recv,
     rp_send,
     rp_recv,
     rm_send,
@@ -141,6 +178,7 @@
     positions = lru.shape[0]
     model = wg.shape[0]
     width = model // PARTS
+    half_w = width // 2
     n_z = n_tp // 2
     hops = n_z // 2
     quads = n_tp // PARTS
@@ -178,6 +216,12 @@
     def cols(part):
         return pl.ds(pl.multiple_of(part * width, LANES), width)
 
+    def z_cols(part):
+        return pl.ds(pl.multiple_of(part * half_w, LANES), half_w)
+
+    def x_cols(core):
+        return pl.ds(pl.multiple_of(PARTS * half_w + core * width, LANES), width)
+
     def rows(start, size):
         return pl.ds(pl.multiple_of(start, 8), size)
 
@@ -192,10 +236,17 @@
         pltpu.make_async_copy(
             resid_hbm.at[rows(q_me * tokens, tokens), cols(p_me)], resid, load_sem.at[1]
         ),
-        pltpu.make_async_copy(wg_hbm, wg, load_sem.at[2]),
-        pltpu.make_async_copy(wu_hbm, wu, load_sem.at[3]),
-        pltpu.make_async_copy(wd_hbm, wd, load_sem.at[4]),
     ]
+    for part in range(PARTS):
+        x_at = PARTS * half_w + (part % 2) * width + (part // 2) * half_w
+        for source, target in ((part * width, part * half_w), (part * width + half_w, x_at)):
+            source, target = pl.ds(source, half_w), pl.ds(target, half_w)
+            for a, b in (
+                (wg_hbm.at[source, :], wg.at[target, :]),
+                (wu_hbm.at[source, :], wu.at[target, :]),
+                (wd_hbm.at[:, source], wd.at[:, target]),
+            ):
+                loads.append(pltpu.make_async_copy(a, b, load_sem.at[len(loads)]))
     for load in loads:
         load.start()
 
@@ -267,6 +318,31 @@
     for d in range(1, n_sp):
         front_copy(d, s_me).start()
     gelu_gain = gelu(gate[...].astype(F32)) * gain[...]
+
+    slots = n_sp * slot_rows
+    shape = (tokens, slots)
+    lane, token = iota(shape, 1), iota(shape, 0)
+    expert = lax.div(lane, slot_rows).astype(F32)
+    place = lax.rem(lane, cap).astype(F32)
+    here = lax.div(lax.rem(lane, slot_rows), cap) == lax.div(token, ROUTE_ROWS)
+    earlier = jnp.where(iota((tokens, tokens), 1) < iota((tokens, tokens), 0), 1.0, 0.0).astype(BF16)
+    route_rows = routes[...].astype(F32)
+    for q in range(quads):
+        named = [
+            here & (column_of(route_rows[k : k + 1, :], q * tokens, tokens) == expert)
+            for k in range(2)
+        ]
+        chosen = jnp.where(named[0] | named[1], 1.0, 0.0)
+        rank = jnp.dot(earlier, chosen.astype(BF16), preferred_element_type=F32)
+        pick = jnp.where(rank == place, chosen, 0.0)
+        weight = jnp.zeros(shape, F32)
+        for k in range(2):
+            own_weight = column_of(rweights[k : k + 1, :], q * tokens, tokens)
+            weight = weight + jnp.where(named[k], own_weight * pick, 0.0)
+        high = weight.astype(BF16)
+        pk[q] = pick.astype(BF16)
+        wh[q] = high
+        wl[q] = (weight - high.astype(F32)).astype(BF16)
     for d in range(1, n_sp):
         front_copy(d, sp_peer(d)).wait_recv()
 
@@ -327,13 +403,16 @@
     for d in range(1, n_tp):
         square_copy(d, t_me).start()
 
-    def to_sibling(src, dst, send, recv, q):
+    def chip_at(offset):
+        return lax.rem(z_me + offset + 2 * n_z, n_z)
+
+    def to_sibling(src, dst, send, recv, q, at):
         copies = []
         for j in range(2):
             chip = 2 * q + j
             copies.append(
                 remote(
-                    src.at[q, :, cols(2 * j + 1 - c_me)],
+                    src.at[q, :, at(2 * j + 1 - c_me)],
                     dst.at[chip],
                     send.at[chip],
                     recv.at[chip],
@@ -342,12 +421,8 @@
             )
         return copies
 
-    def reduce_scatter(src, sib_buf, stage, buf_p, buf_m, sems, half):
+    def reduce_scatter(src, sib_buf, stage, buf_p, buf_m, sems, half, column):
         sib_s, sib_r, p_s, p_r, m_s, m_r = sems
-        arrived = []
-
-        def chip_at(offset):
-            return lax.rem(z_me + offset + 2 * n_z, n_z)
 
         def wait_sibling(chip):
             remote(
@@ -356,7 +431,7 @@
 
         def term(chip, h):
             at = pl.ds(h * half, half)
-            mine = src[lax.div(chip, 2), at, cols(lax.rem(chip, 2) * 2 + c_me)]
+            mine = src[lax.div(chip, 2), at, column(lax.rem(chip, 2) * 2 + c_me)]
             return mine.astype(F32) + sib_buf[chip, at, :].astype(F32)
 
         def length(direction, h):
@@ -375,22 +450,24 @@
             return buf.at[h, j - 1]
 
         lanes = [(1, 0), (-1, 1), (1, 1), (-1, 0)]
-        wait_sibling(chip_at(hops))
-        for n, (direction, h) in enumerate(lanes):
-            if n == 2:
-                wait_sibling(chip_at(hops - 1))
-                if hops > 1:
-                    wait_sibling(chip_at(1 - hops))
-            if length(direction, h) == 0:
-                continue
-            stage[n] = term(chip_at(direction * length(direction, h)), h).astype(BF16)
-            hop(direction, h, 1, stage.at[n]).start()
-        for d in range(hops - 2, -1, -1):
-            wait_sibling(chip_at(d))
-            if d > 0:
-                wait_sibling(chip_at(-d))
-
-        def step_of(j, _):
+
+        def begin():
+            wait_sibling(chip_at(hops))
+            for n, (direction, h) in enumerate(lanes):
+                if n == 2:
+                    wait_sibling(chip_at(hops - 1))
+                    if hops > 1:
+                        wait_sibling(chip_at(1 - hops))
+                if length(direction, h) == 0:
+                    continue
+                stage[n] = term(chip_at(direction * length(direction, h)), h).astype(BF16)
+                hop(direction, h, 1, stage.at[n]).start()
+            for d in range(hops - 2, -1, -1):
+                wait_sibling(chip_at(d))
+                if d > 0:
+                    wait_sibling(chip_at(-d))
+
+        def step_of(j):
             for direction, h in lanes:
                 n = length(direction, h)
 
@@ -401,14 +478,9 @@
                     slot[...] = value.astype(BF16)
                     hop(direction, h, j, slot).start()
 
-                if n == hops:
-                    one()
-                else:
-                    pl.when(j < hops)(one)
-            return 0
-
-        lax.fori_loop(2, hops + 1, step_of, 0)
-        for h in range(2):
+                when(j <= n if isinstance(j, int) else n == hops or j <= n, one)
+
+        def result(h):
             total = term(z_me, h)
             for direction in (1, -1):
                 n = length(direction, h)
@@ -416,18 +488,21 @@
                     slot = arrival(direction, h, n)
                     hop(direction, h, n, slot).wait_recv()
                     total = total + slot[...].astype(F32)
-            arrived.append(total)
-        for n, (direction, h) in enumerate(lanes):
-            for j in range(1, length(direction, h) + 1):
-                hop(direction, h, j, arrival(direction, h, j)).wait_send()
-        return arrived
+            return total
+
+        def drain():
+            for n, (direction, h) in enumerate(lanes):
+                for j in range(1, length(direction, h) + 1):
+                    hop(direction, h, j, arrival(direction, h, j)).wait_send()
+
+        return begin, step_of, result, drain
 
     copies = []
     for q in range(quads):
-        copies += to_sibling(pp, psib, psib_send, psib_recv, q)
+        copies += to_sibling(pp, psib, psib_send, psib_recv, q, cols)
     for copy in copies:
         copy.start()
-    parts = reduce_scatter(
+    begin, step_of, result, drain_projection = reduce_scatter(
         pp,
         psib,
         pst,
@@ -435,9 +510,16 @@
         prm,
         (psib_send, psib_recv, prp_send, prp_recv, prm_send, prm_recv),
         half_tokens,
+        cols,
     )
-    for copy in copies:
-        copy.wait_send()
+    begin()
+
+    def projection_step(j, _):
+        step_of(j)
+        return 0
+
+    lax.fori_loop(2, hops + 1, projection_step, 0)
+    parts = [result(h) for h in range(2)]
     for d in range(1, n_tp):
         square_copy(d, tp_peer(d)).wait_recv()
     squares = sqb[0]
@@ -471,45 +553,56 @@
     for d in range(1, PARTS):
         norm_copy(d, p_me).start()
 
-    slots = n_sp * slot_rows
-    shape = (tokens, slots)
-    lane, token = iota(shape, 1), iota(shape, 0)
-    expert = lax.div(lane, slot_rows)
-    block = lax.div(lax.rem(lane, slot_rows), cap)
-    place = lax.rem(lane, cap).astype(F32)
-    here = block == lax.div(token, ROUTE_ROWS)
-    expert = expert.astype(F32)
-    route_rows = routes[...].astype(F32)
-    named = [
-        here & (column_of(route_rows[k : k + 1, :], q_me * tokens, tokens) == expert)
-        for k in range(2)
-    ]
-    chosen = jnp.where(named[0] | named[1], 1.0, 0.0)
-    earlier = jnp.where(iota((tokens, tokens), 1) < iota((tokens, tokens), 0), 1.0, 0.0)
-    rank = jnp.dot(earlier.astype(BF16), chosen.astype(BF16), preferred_element_type=F32)
-    pick = jnp.where(rank == place, chosen, 0.0)
-    weight = jnp.zeros(shape, F32)
-    for k in range(2):
-        own_weight = column_of(rweights[k : k + 1, :], q_me * tokens, tokens)
-        weight = weight + jnp.where(named[k], own_weight * pick, 0.0)
-    weight_high = weight.astype(BF16)
-    weight_low = (weight - weight_high.astype(F32)).astype(BF16)
     scale = fgain[:, cols(p_me)]
     for d in range(1, PARTS):
         norm_copy(d, quad_peer(d)).wait_recv()
     squares = sq2[0] + sq2[1] + sq2[2] + sq2[3]
     inverse = column_of(lax.rsqrt(squares / model + EPSILON), 0, tokens)
     normed = (after * inverse * scale).astype(BF16)
+    turn = 2 * lax.rem(z_me, 2) - 1
+
+    def quad_at(k):
+        far = lax.div(k, 2)
+        offset = jnp.where(lax.rem(k, 2) == 0, turn * far, -turn * far)
+        return lax.rem(q_me + offset + 2 * quads, quads)
+
+    xa[z_me] = normed[:, half_w:]
+
+    def ahead_copy(direction, k, chip):
+        sends, recvs = (xap_send, xap_recv) if direction > 0 else (xam_send, xam_recv)
+        return remote(
+            xa.at[chip],
+            xa.at[chip],
+            sends.at[k],
+            recvs.at[k],
+            tp=up if direction > 0 else down,
+        )
+
+    def ahead_step(k):
+        for direction, n in ((1, hops), (-1, hops - 1)):
+
+            def arrive(direction=direction, n=n):
+                chip = chip_at(-direction * k)
+                ahead_copy(direction, k - 1, chip).wait_recv()
+                when(k < n, lambda: ahead_copy(direction, k, chip).start())
+
+            when(k <= n, arrive)
+
+    ahead_copy(1, 0, z_me).start()
+    if hops > 1:
+        ahead_copy(-1, 0, z_me).start()
+
+    over_slots = (((0,), (0,)), ((), ()))
     outgoing = lax.dot_general(
-        pick.astype(BF16), normed, (((0,), (0,)), ((), ())), preferred_element_type=F32
+        pk[q_me], normed[:, :half_w], over_slots, preferred_element_type=F32
     ).astype(BF16)
-    og[...] = outgoing.reshape(n_sp, slot_rows, width)
-    xg[q_me, rows(s_me * slot_rows, slot_rows), cols(p_me)] = og[s_me]
+    og[...] = outgoing.reshape(n_sp, slot_rows, half_w)
+    xg[q_me, rows(s_me * slot_rows, slot_rows), z_cols(p_me)] = og[s_me]
 
     def dispatch_copy(d, source, peer):
         return remote(
             og.at[peer],
-            xg.at[q_me, rows(source * slot_rows, slot_rows), cols(p_me)],
+            xg.at[q_me, rows(source * slot_rows, slot_rows), z_cols(p_me)],
             di_send.at[d],
             di_recv.at[source],
             sp=peer,
@@ -517,12 +610,33 @@
 
     for d in range(1, n_sp):
         dispatch_copy(d, s_me, sp_peer(d)).start()
+
+    def late_copy(q, d, source, peer):
+        return remote(
+            ox.at[q, peer],
+            xg.at[q, rows(source * slot_rows, slot_rows), x_cols(c_me)],
+            ox_send.at[q, d],
+            ox_recv.at[q, source],
+            sp=peer,
+        )
+
+    def send_quad(q):
+        both = jnp.concatenate([xa[2 * q], xa[2 * q + 1]], axis=1)
+        picked = lax.dot_general(pk[q], both, over_slots, preferred_element_type=F32)
+        ox[q] = picked.astype(BF16).reshape(n_sp, slot_rows, width)
+        xg[q, rows(s_me * slot_rows, slot_rows), x_cols(c_me)] = ox[q, s_me]
+
+        def one(d, _):
+            late_copy(q, d, s_me, sp_peer(d)).start()
+            return 0
+
+        lax.fori_loop(1, n_sp, one, 0)
 
     def sub_block(chip, h, core):
         return xg.at[
             lax.div(chip, 2),
             pl.ds(h * half_slots, half_slots),
-            cols(lax.rem(chip, 2) * 2 + core),
+            z_cols(lax.rem(chip, 2) * 2 + core),
         ]
 
     def ring_copy(direction, h, k, chip):
@@ -536,34 +650,37 @@
         view = sub_block(chip, h, core)
         return remote(view, view, ags_send.at[h, chip], ags_recv.at[h, chip], tp=sibling)
 
+    def across_late(q, core):
+        view = xg.at[q, :, x_cols(core)]
+        return remote(view, view, xf_send.at[q], xf_recv.at[q], tp=sibling)
+
     def reach(direction, h):
         return hops if (direction > 0) == (h == 0) else hops - 1
 
+    ahead_step(1)
+    send_quad(quad_at(1))
+    ahead_step(2)
+    send_quad(quad_at(2))
     for h in range(2):
         for source in range(h * n_sp // 2, (h + 1) * n_sp // 2):
+
             @pl.when(source != s_me)
             def _(source=source):
-                remote(
-                    og.at[source],
-                    xg.at[q_me, rows(source * slot_rows, slot_rows), cols(p_me)],
-                    di_send.at[0],
-                    di_recv.at[source],
-                    sp=sp_peer(1),
-                ).wait_recv()
+                dispatch_copy(0, source, source).wait_recv()
+
         for direction in (1, -1):
             if reach(direction, h):
                 ring_copy(direction, h, 0, z_me).start()
         across_copy(h, z_me, c_me).start()
     for load in loads[2:]:
         load.wait()
-    turn = 2 * lax.rem(z_me, 2) - 1
-
-    def gather_step(k, _):
-        for direction, h in ((1, 0), (-1, 1), (1, 1), (-1, 0)):
+
+    def forward(k, h):
+        for direction in (1, -1) if h == 0 else (-1, 1):
             n = reach(direction, h)
 
-            def arrive(direction=direction, h=h, n=n):
-                chip = lax.rem(z_me - direction * k + 2 * n_z, n_z)
+            def arrive(direction=direction, n=n):
+                chip = chip_at(-direction * k)
                 ring_copy(direction, h, k - 1, chip).wait_recv()
 
                 @pl.when(k < n)
@@ -572,30 +689,142 @@
 
                 across_copy(h, chip, c_me).start()
 
-            if n == hops:
-                arrive()
-            else:
-                pl.when(k < hops)(arrive)
-        far = lax.div(k, 2)
-        offset = jnp.where(lax.rem(k, 2) == 0, turn * far, -turn * far)
-        q = lax.rem(q_me + offset + 2 * quads, quads)
+            pl.when(k <= n)(arrive)
+
+    def forward_late(q):
+        def one(d, _):
+            late_copy(q, 0, sp_peer(d), sp_peer(d)).wait_recv()
+            return 0
+
+        lax.fori_loop(1, n_sp, one, 0)
+        across_late(q, c_me).start()
+
+    def late_to_sibling(q):
+        return remote(
+            po.at[q, :, x_cols(1 - c_me)],
+            xsib.at[q],
+            xsib_send.at[q],
+            xsib_recv.at[q],
+            tp=sibling,
+        )
+
+    def out_to_sibling(q):
+        return [late_to_sibling(q)] + to_sibling(po, sib, sib_send, sib_recv, q, z_cols)
+
+    def experts_gate(q):
         for j in range(2):
             for h in range(2):
                 across_copy(h, 2 * q + j, 1 - c_me).wait_recv()
-        rows_in = xg[q]
-        gate_part = jnp.dot(rows_in, wg[...], preferred_element_type=F32)
-        up_part = jnp.dot(rows_in, wu[...], preferred_element_type=F32)
-        units = (jax.nn.silu(gate_part) * up_part).astype(BF16)
+        across_late(q, 1 - c_me).wait_recv()
+        gs[...] = jax.nn.silu(jnp.dot(xg[q], wg[...], preferred_element_type=F32))
+
+    def experts(q):
+        up_part = jnp.dot(xg[q], wu[...], preferred_element_type=F32)
+        units = (gs[...] * up_part).astype(BF16)
         for part in range(PARTS):
             at = slice(part * width, (part + 1) * width)
             po[q, :, at] = jnp.dot(units, wd[:, at], preferred_element_type=F32).astype(BF16)
-        for copy in to_sibling(po, sib, sib_send, sib_recv, q):
+        for copy in out_to_sibling(q):
             copy.start()
+
+    def early_copy(q, d, source, peer):
+        return remote(
+            xo.at[q, peer], xi.at[q, source], xo_send.at[q, d], xo_recv.at[q, source], sp=peer
+        )
+
+    def return_early(q):
+        late_to_sibling(q).wait_recv()
+        total = po[q, :, x_cols(c_me)].astype(F32) + xsib[q].astype(F32)
+        xo[q] = total.astype(BF16).reshape(n_sp, slot_rows, width)
+        xi[q, pl.ds(s_me, 1)] = xo[q, pl.ds(s_me, 1)]
+
+        def one(d, _):
+            early_copy(q, d, s_me, sp_peer(d)).start()
+            return 0
+
+        lax.fori_loop(1, n_sp, one, 0)
+
+    def weigh(q, back):
+        return jnp.dot(wh[q], back, preferred_element_type=F32) + jnp.dot(
+            wl[q], back, preferred_element_type=F32
+        )
+
+    def weigh_early(q):
+        def one(d, _):
+            early_copy(q, 0, sp_peer(d), sp_peer(d)).wait_recv()
+            return 0
+
+        lax.fori_loop(1, n_sp, one, 0)
+        total = weigh(q, xi[q].reshape(slots, width))
+        for j in range(2):
+            co[2 * q + j] = total[:, j * half_w : (j + 1) * half_w]
+
+    def home_copy(direction, j, source):
+        sends, recvs, slot = (hp_send, hp_recv, hp) if direction > 0 else (hm_send, hm_recv, hm)
+        return remote(
+            source,
+            slot.at[j - 1],
+            sends.at[j - 1],
+            recvs.at[j - 1],
+            tp=up if direction > 0 else down,
+        )
+
+    ways = [(1, hops, hp), (-1, hops - 1, hm)]
+
+    def home_step(j):
+        for direction, n, slots_in in ways:
+            if j > n:
+                continue
+            value = co[chip_at(direction * (n + 1 - j))]
+            if j == 1:
+                source = hs_out.at[0 if direction > 0 else 1]
+            else:
+                source = slots_in.at[j - 2]
+                home_copy(direction, j - 1, source).wait_recv()
+                value = value + source[...].astype(F32)
+            source[...] = value.astype(BF16)
+            home_copy(direction, j, source).start()
+
+    def home_result():
+        total = co[z_me]
+        for direction, n, slots_in in ways:
+            if n:
+                home_copy(direction, n, slots_in.at[n - 1]).wait_recv()
+                total = total + slots_in[n - 1].astype(F32)
+        return total
+
+    def gather_step(k, _):
+        @pl.when(k <= hops - 2)
+        def _():
+            ahead_step(k + 2)
+            send_quad(quad_at(k + 2))
+
+        @pl.when(k <= hops)
+        def _():
+            forward(k, 0)
+
+        @pl.when(k >= 2)
+        def _():
+            experts_gate(quad_at(k - 1))
+
+        @pl.when(k <= hops)
+        def _():
+            forward(k, 1)
+            forward_late(quad_at(k))
+
+        @pl.when(k >= 2)
+        def _():
+            experts(quad_at(k - 1))
+
+        @pl.when(k >= 3)
+        def _():
+            return_early(quad_at(k - 2))
+
         return 0
 
-    lax.fori_loop(1, hops + 1, gather_step, 0)
-
-    parts = reduce_scatter(
+    lax.fori_loop(1, hops + 2, gather_step, 0)
+
+    begin, step_of, result, drain_experts = reduce_scatter(
         po,
         sib,
         st,
@@ -603,28 +832,52 @@
         rm,
         (sib_send, sib_recv, rp_send, rp_recv, rm_send, rm_recv),
         half_slots,
+        z_cols,
     )
+    begin()
+    return_early(quad_at(hops))
+
+    homeward = 0
+    for j in range(2, hops + 1):
+        step_of(j)
+        if homeward:
+            homeward += 1
+            home_step(homeward)
+        for k in range(2 * j - 3, min(2 * j - 1, hops + 1)):
+            weigh_early(quad_at(k))
+            if k == hops:
+                homeward = 1
+                home_step(1)
     half_sp = n_sp // 2
-    for h in range(2):
-        ret[h * half_sp : (h + 1) * half_sp] = (
-            parts[h].astype(BF16).reshape(half_sp, slot_rows, width)
-        )
-    rt[pl.ds(s_me, 1)] = ret[pl.ds(s_me, 1)]
 
     def return_copy(d, source, peer):
         return remote(
             ret.at[peer], rt.at[source], ret_send.at[d], ret_recv.at[source], sp=peer
         )
 
+    for h in range(2):
+        ret[h * half_sp : (h + 1) * half_sp] = (
+            result(h).astype(BF16).reshape(half_sp, slot_rows, half_w)
+        )
+    rt[pl.ds(s_me, 1)] = ret[pl.ds(s_me, 1)]
     for d in range(1, n_sp):
         return_copy(d, s_me, sp_peer(d)).start()
+    for j in range(homeward + 1, hops + 1):
+        home_step(j)
     for d in range(1, n_sp):
         return_copy(d, sp_peer(d), sp_peer(d)).wait_recv()
-    back = rt[...].reshape(slots, width)
-    routed = jnp.dot(weight_high, back, preferred_element_type=F32) + jnp.dot(
-        weight_low, back, preferred_element_type=F32
+    routed = weigh(q_me, rt[...].reshape(slots, half_w))
+    fo[:, :, :half_w] = (
+        (resid[:, :half_w].astype(F32) + routed)
+        .astype(BF16)
+        .reshape(PARTS, ROUTE_ROWS, half_w)
     )
-    fo[...] = (resid[...].astype(F32) + routed).astype(BF16).reshape(PARTS, ROUTE_ROWS, width)
+    routed = home_result()
+    fo[:, :, half_w:] = (
+        (resid[:, half_w:].astype(F32) + routed)
+        .astype(BF16)
+        .reshape(PARTS, ROUTE_ROWS, half_w)
+    )
     fin[pl.ds(p_me, 1)] = fo[pl.ds(p_me, 1)]
 
     def final_copy(d, source, peer):
@@ -658,10 +911,25 @@
                 ring_copy(direction, h, k, z_me).wait_send()
         for chip in range(n_z):
             across_copy(h, chip, c_me).wait_send()
+    for copy in copies:
+        copy.wait_send()
+    drain_projection()
+    drain_experts()
+    for direction, n, slots_in in ways:
+        for k in range(n):
+            ahead_copy(direction, k, z_me).wait_send()
+            home_copy(direction, k + 1, slots_in.at[k]).wait_send()
     for q in range(quads):
-        for copy in to_sibling(po, sib, sib_send, sib_recv, q):
+        across_late(q, c_me).wait_send()
+        for copy in out_to_sibling(q):
             copy.wait_send()
 
+        def one(d, _, q=q):
+            late_copy(q, d, s_me, sp_peer(d)).wait_send()
+            early_copy(q, d, s_me, sp_peer(d)).wait_send()
+            return 0
+
+        lax.fori_loop(1, n_sp, one, 0)
 
 def local(
     n_sp,
@@ -687,6 +955,7 @@
     model = residual.shape[1]
     units = w_gate.shape[2]
     width = model // PARTS
+    half_w = width // 2
     n_z = n_tp // 2
     hops = n_z // 2
     quads = n_tp // PARTS
@@ -719,18 +988,31 @@
         pltpu.VMEM((4, tokens // 2, width), BF16),
         pltpu.VMEM((2, hops, tokens // 2, width), BF16),
         pltpu.VMEM((2, hops, tokens // 2, width), BF16),
-        pltpu.VMEM((n_sp, slot_rows, width), BF16),
+        pltpu.VMEM((quads, tokens, block_rows), BF16),
+        pltpu.VMEM((quads, tokens, block_rows), BF16),
+        pltpu.VMEM((quads, tokens, block_rows), BF16),
+        pltpu.VMEM((n_sp, slot_rows, half_w), BF16),
+        pltpu.VMEM((n_z, tokens, half_w), BF16),
+        pltpu.VMEM((quads, n_sp, slot_rows, width), BF16),
         pltpu.VMEM((quads, block_rows, model), BF16),
         pltpu.VMEM((quads, block_rows, model), BF16),
-        pltpu.VMEM((n_z, block_rows, width), BF16),
-        pltpu.VMEM((4, block_rows // 2, width), BF16),
-        pltpu.VMEM((2, hops, block_rows // 2, width), BF16),
-        pltpu.VMEM((2, hops, block_rows // 2, width), BF16),
-        pltpu.VMEM((n_sp, slot_rows, width), BF16),
-        pltpu.VMEM((n_sp, slot_rows, width), BF16),
+        pltpu.VMEM((n_z, block_rows, half_w), BF16),
+        pltpu.VMEM((quads, block_rows, width), BF16),
+        pltpu.VMEM((quads, n_sp, slot_rows, width), BF16),
+        pltpu.VMEM((quads, n_sp, slot_rows, width), BF16),
+        pltpu.VMEM((n_z, tokens, half_w), F32),
+        pltpu.VMEM((2, tokens, half_w), BF16),
+        pltpu.VMEM((hops, tokens, half_w), BF16),
+        pltpu.VMEM((hops, tokens, half_w), BF16),
+        pltpu.VMEM((block_rows, units), F32),
+        pltpu.VMEM((4, block_rows // 2, half_w), BF16),
+        pltpu.VMEM((2, hops, block_rows // 2, half_w), BF16),
+        pltpu.VMEM((2, hops, block_rows // 2, half_w), BF16),
+        pltpu.VMEM((n_sp, slot_rows, half_w), BF16),
+        pltpu.VMEM((n_sp, slot_rows, half_w), BF16),
         pltpu.VMEM((PARTS, ROUTE_ROWS, width), BF16),
         pltpu.VMEM((PARTS, ROUTE_ROWS, width), BF16),
-        dma((5,)),
+        dma((2 + 6 * PARTS,)),
         dma((n_sp,)),
         dma((n_sp,)),
         dma((n_tp,)),
@@ -751,8 +1033,24 @@
         dma((2, hops)),
         dma((2, n_z)),
         dma((2, n_z)),
+        dma((hops,)),
+        dma((hops,)),
+        dma((hops,)),
+        dma((hops,)),
+        dma((quads, n_sp)),
+        dma((quads, n_sp)),
+        dma((quads,)),
+        dma((quads,)),
         dma((n_z,)),
         dma((n_z,)),
+        dma((quads,)),
+        dma((quads,)),
+        dma((quads, n_sp)),
+        dma((quads, n_sp)),
+        dma((hops,)),
+        dma((hops,)),
+        dma((hops,)),
+        dma((hops,)),
         dma((2, hops)),
         dma((2, hops)),
         dma((2, hops)),

time: 104 us -> 98.7 us (0.949)
  Pallas kernels: 103 us -> 97 us
    pallas_call x1, Pallas kernels: 103 us -> 97 us  [local(): pl.pallas_call(functools.partial(kernel, n_sp, n_tp), out_shape=jax.Shape...]
where the time goes in v2:
time: 98.7 us; the launch traced here: 98.5 us
  Pallas kernels  97 us (98%)
  local copies, waits for them, and re-layouts  1.47 us (1%)
    pallas_call x1, Pallas kernels, local(): pl.pallas_call(functools.partial(kernel, n_sp, n_tp), out_shape=jax.Shape...  97 us

profile of v2, /device:TPU:1, one launch (start us, length us, event | category | flops | bytes accessed | tf_op | source)
XLA Modules:
  0.0 98.5 jit_solution(1345966166161645688)
XLA Ops:
  0.0 97.0 %layer.1 = bf16[16,2048]{1,0:T(8,128)(2,1)} custom-call(bf16[256,128]{1,0:T(8,128)(2,1)} %lru.1, bf16[256,128]{1,0:T(8,128)(2,1)} %gate.1, s32[1,256]{1,0:T(1,128)} %bitcast.19, bf16[4,128]{1,0:T(4,128)(2,1)} %taps.1, bf16[128,128]{1,0:T(8,128)(2,1)} %bitcast.14, bf16[128,128]{1,0:T(8,128)(2,1)} %bitcast.15, f32[1,128]{1,0:T(1,128)} %bitcast.20, ...), custom_call_target="tpu_custom_call" | custom-call | tf_op jit(solution)/shard_map/layer/pallas_call | solution.py:1063
  97.0 1.5 %copy.18 = bf16[16,2048]{1,0:T(8,128)(2,1)} copy(bf16[16,2048]{1,0:T(8,128)(2,1)} %layer.1) | data formatting | bytes 131072

commit v3 on v2

--- a/solution.py
+++ b/solution.py
@@ -16,6 +16,7 @@
 LANES = 128
 REACH = 3
 ROUTE_ROWS = 16
+PIECES = 4
 
 
 def softplus_of_minus(v):
@@ -66,6 +67,23 @@
 def kernel(
     n_sp,
     n_tp,
+    lru_hbm,
+    gate_hbm,
+    docs_hbm,
+    taps_hbm,
+    rate_hbm,
+    inlet_hbm,
+    decay_hbm,
+    gain_hbm,
+    fgain_hbm,
+    routes_hbm,
+    rweights_hbm,
+    w_out_hbm,
+    resid_hbm,
+    wg_hbm,
+    wu_hbm,
+    wd_hbm,
+    out,
     lru,
     gate,
     docs,
@@ -77,12 +95,7 @@
     fgain,
     routes,
     rweights,
-    w_out_hbm,
-    resid_hbm,
-    wg_hbm,
-    wu_hbm,
-    wd_hbm,
-    out,
+    in_sem,
     xs,
     ds,
     a_s,
@@ -93,8 +106,7 @@
     hd,
     w_out,
     resid,
-    wg,
-    wu,
+    wgu,
     wd,
     sqb,
     sq2,
@@ -116,9 +128,7 @@
     xo,
     xi,
     co,
-    hs_out,
-    hp,
-    hm,
+    ci,
     gs,
     st,
     rp,
@@ -154,18 +164,14 @@
     xam_recv,
     ox_send,
     ox_recv,
-    xf_send,
-    xf_recv,
     sib_send,
     sib_recv,
     xsib_send,
     xsib_recv,
     xo_send,
     xo_recv,
-    hp_send,
-    hp_recv,
-    hm_send,
-    hm_recv,
+    co_send,
+    co_recv,
     rp_send,
     rp_recv,
     rm_send,
@@ -176,7 +182,8 @@
     fin_recv,
 ):
     positions = lru.shape[0]
-    model = wg.shape[0]
+    model = wgu.shape[0]
+    units_n = wd.shape[0]
     width = model // PARTS
     half_w = width // 2
     n_z = n_tp // 2
@@ -185,7 +192,7 @@
     tokens = positions // quads
     slot_rows = rt.shape[1]
     cap = slot_rows // PARTS
-    half_slots = n_sp * slot_rows // 2
+    piece_slots = n_sp * slot_rows // PIECES
     half_tokens = tokens // 2
     s_me = lax.axis_index("sp")
     t_me = lax.axis_index("tp")
@@ -213,6 +220,12 @@
             device_id_type=MESH,
         )
 
+    def got(view, sem):
+        remote(view, view, sem, sem, tp=sibling).wait_recv()
+
+    def sent(view, sem):
+        remote(view, view, sem, sem, tp=sibling).wait_send()
+
     def cols(part):
         return pl.ds(pl.multiple_of(part * width, LANES), width)
 
@@ -225,6 +238,21 @@
     def rows(start, size):
         return pl.ds(pl.multiple_of(start, 8), size)
 
+    inputs = [
+        pltpu.make_async_copy(lru_hbm, lru, in_sem.at[0]),
+        pltpu.make_async_copy(gate_hbm, gate, in_sem.at[1]),
+        pltpu.make_async_copy(docs_hbm, docs, in_sem.at[2]),
+        pltpu.make_async_copy(taps_hbm, taps, in_sem.at[3]),
+        pltpu.make_async_copy(rate_hbm, rate, in_sem.at[4]),
+        pltpu.make_async_copy(inlet_hbm, inlet, in_sem.at[5]),
+        pltpu.make_async_copy(decay_hbm, decay, in_sem.at[6]),
+        pltpu.make_async_copy(gain_hbm, gain, in_sem.at[7]),
+        pltpu.make_async_copy(fgain_hbm, fgain, in_sem.at[8]),
+        pltpu.make_async_copy(routes_hbm, routes, in_sem.at[9]),
+        pltpu.make_async_copy(rweights_hbm, rweights, in_sem.at[10]),
+    ]
+    for copy in inputs:
+        copy.start()
     barrier = pltpu.get_barrier_semaphore()
     for d in range(1, n_sp):
         pl.semaphore_signal(barrier, inc=1, device_id={"sp": sp_peer(d)}, device_id_type=MESH)
@@ -242,11 +270,15 @@
         for source, target in ((part * width, part * half_w), (part * width + half_w, x_at)):
             source, target = pl.ds(source, half_w), pl.ds(target, half_w)
             for a, b in (
-                (wg_hbm.at[source, :], wg.at[target, :]),
-                (wu_hbm.at[source, :], wu.at[target, :]),
-                (wd_hbm.at[:, source], wd.at[:, target]),
+                (wg_hbm.at[source, :], wgu.at[target, pl.ds(0, units_n)]),
+                (wu_hbm.at[source, :], wgu.at[target, pl.ds(units_n, units_n)]),
             ):
-                loads.append(pltpu.make_async_copy(a, b, load_sem.at[len(loads)]))
+                loads.append(pltpu.make_async_copy(a, b, load_sem.at[2]))
+            loads.append(
+                pltpu.make_async_copy(wd_hbm.at[:, source], wd.at[:, target], load_sem.at[3])
+            )
+    for copy in inputs:
+        copy.wait()
     for load in loads:
         load.start()
 
@@ -313,7 +345,7 @@
 
     def front_copy(d, source):
         block = rx.at[rows((source + 1) * 16, 16), :]
-        return remote(block, block, fr_send.at[d], fr_recv.at[source], sp=sp_peer(d))
+        return remote(block, block, fr_send, fr_recv, sp=sp_peer(d))
 
     for d in range(1, n_sp):
         front_copy(d, s_me).start()
@@ -343,8 +375,7 @@
         pk[q] = pick.astype(BF16)
         wh[q] = high
         wl[q] = (weight - high.astype(F32)).astype(BF16)
-    for d in range(1, n_sp):
-        front_copy(d, sp_peer(d)).wait_recv()
+    got(rx.at[: (n_sp - 1) * 16, :], fr_recv)
 
     seq = [rx[pl.ds(5 + k, n_sp, stride=16), :] for k in range(REACH)]
     seq += [rx[pl.ds(18 + k, n_sp, stride=16), :] for k in range(REACH)]
@@ -389,7 +420,7 @@
 
     def square_copy(d, source):
         return remote(
-            sqb.at[source], sqb.at[source], sq_send.at[d], sq_recv.at[source], tp=tp_peer(d)
+            sqb.at[source], sqb.at[source], sq_send, sq_recv, tp=tp_peer(d)
         )
 
     mixer = (hidden * gelu_gain).astype(BF16)
@@ -414,20 +445,16 @@
                 remote(
                     src.at[q, :, at(2 * j + 1 - c_me)],
                     dst.at[chip],
-                    send.at[chip],
-                    recv.at[chip],
+                    send,
+                    recv.at[q],
                     tp=sibling,
                 )
             )
         return copies
 
-    def reduce_scatter(src, sib_buf, stage, buf_p, buf_m, sems, half, column):
-        sib_s, sib_r, p_s, p_r, m_s, m_r = sems
-
-        def wait_sibling(chip):
-            remote(
-                sib_buf.at[chip], sib_buf.at[chip], sib_s.at[chip], sib_r.at[chip], tp=sibling
-            ).wait_recv()
+    def reduce_scatter(src, sib_buf, stage, buf_p, buf_m, sems, pieces, column):
+        sib_r, p_s, p_r, m_s, m_r = sems
+        half = src.shape[1] // pieces
 
         def term(chip, h):
             at = pl.ds(h * half, half)
@@ -435,37 +462,33 @@
             return mine.astype(F32) + sib_buf[chip, at, :].astype(F32)
 
         def length(direction, h):
-            return hops if (direction > 0) == (h == 0) else hops - 1
+            return hops if (direction > 0) == (h % 2 == 0) else hops - 1
 
         def hop(direction, h, j, source):
             buf = buf_p if direction > 0 else buf_m
             sends, recvs = (p_s, p_r) if direction > 0 else (m_s, m_r)
             target = up if direction > 0 else down
             return remote(
-                source, buf.at[h, j - 1], sends.at[h, j - 1], recvs.at[h, j - 1], tp=target
+                source, buf.at[h * hops + j - 1], sends, recvs.at[h, j - 1], tp=target
             )
 
         def arrival(direction, h, j):
             buf = buf_p if direction > 0 else buf_m
-            return buf.at[h, j - 1]
-
-        lanes = [(1, 0), (-1, 1), (1, 1), (-1, 0)]
+            return buf.at[h * hops + j - 1]
+
+        lanes = [(1 - 2 * (h % 2), h) for h in range(pieces)]
+        lanes += [(2 * (h % 2) - 1, h) for h in range(pieces)]
+        lanes = [lane for h in range(pieces) for lane in (lanes[h], lanes[h + pieces])]
+        lanes.sort(key=lambda lane: (lane[1] // 2, -length(*lane)))
 
         def begin():
-            wait_sibling(chip_at(hops))
+            for q in range(quads):
+                got(sib_buf.at[2 * q : 2 * q + 2], sib_r.at[q])
             for n, (direction, h) in enumerate(lanes):
-                if n == 2:
-                    wait_sibling(chip_at(hops - 1))
-                    if hops > 1:
-                        wait_sibling(chip_at(1 - hops))
                 if length(direction, h) == 0:
                     continue
                 stage[n] = term(chip_at(direction * length(direction, h)), h).astype(BF16)
                 hop(direction, h, 1, stage.at[n]).start()
-            for d in range(hops - 2, -1, -1):
-                wait_sibling(chip_at(d))
-                if d > 0:
-                    wait_sibling(chip_at(-d))
 
         def step_of(j):
             for direction, h in lanes:
@@ -491,9 +514,10 @@
             return total
 
         def drain():
-            for n, (direction, h) in enumerate(lanes):
-                for j in range(1, length(direction, h) + 1):
-                    hop(direction, h, j, arrival(direction, h, j)).wait_send()
+            for way, buf, sends in ((1, buf_p, p_s), (-1, buf_m, m_s)):
+                count = sum(length(way, h) for h in range(pieces))
+                if count:
+                    sent(buf.at[:count], sends)
 
         return begin, step_of, result, drain
 
@@ -508,8 +532,8 @@
         pst,
         prp,
         prm,
-        (psib_send, psib_recv, prp_send, prp_recv, prm_send, prm_recv),
-        half_tokens,
+        (psib_recv, prp_send, prp_recv, prm_send, prm_recv),
+        2,
         cols,
     )
     begin()
@@ -520,8 +544,7 @@
 
     lax.fori_loop(2, hops + 1, projection_step, 0)
     parts = [result(h) for h in range(2)]
-    for d in range(1, n_tp):
-        square_copy(d, tp_peer(d)).wait_recv()
+    got(sqb.at[: n_tp - 1], sq_recv)
     squares = sqb[0]
     for t in range(1, n_tp):
         squares = squares + sqb[t]
@@ -545,8 +568,8 @@
         return remote(
             sq2.at[source],
             sq2.at[source],
-            s2_send.at[d],
-            s2_recv.at[source],
+            s2_send,
+            s2_recv,
             tp=q_me * PARTS + quad_peer(d),
         )
 
@@ -554,8 +577,7 @@
         norm_copy(d, p_me).start()
 
     scale = fgain[:, cols(p_me)]
-    for d in range(1, PARTS):
-        norm_copy(d, quad_peer(d)).wait_recv()
+    got(sq2.at[: PARTS - 1], s2_recv)
     squares = sq2[0] + sq2[1] + sq2[2] + sq2[3]
     inverse = column_of(lax.rsqrt(squares / model + EPSILON), 0, tokens)
     normed = (after * inverse * scale).astype(BF16)
@@ -573,7 +595,7 @@
         return remote(
             xa.at[chip],
             xa.at[chip],
-            sends.at[k],
+            sends,
             recvs.at[k],
             tp=up if direction > 0 else down,
         )
@@ -603,8 +625,8 @@
         return remote(
             og.at[peer],
             xg.at[q_me, rows(source * slot_rows, slot_rows), z_cols(p_me)],
-            di_send.at[d],
-            di_recv.at[source],
+            di_send,
+            di_recv.at[lax.div(source, n_sp // PIECES)],
             sp=peer,
         )
 
@@ -615,8 +637,8 @@
         return remote(
             ox.at[q, peer],
             xg.at[q, rows(source * slot_rows, slot_rows), x_cols(c_me)],
-            ox_send.at[q, d],
-            ox_recv.at[q, source],
+            ox_send.at[q],
+            ox_recv.at[q],
             sp=peer,
         )
 
@@ -635,7 +657,7 @@
     def sub_block(chip, h, core):
         return xg.at[
             lax.div(chip, 2),
-            pl.ds(h * half_slots, half_slots),
+            pl.ds(h * piece_slots, piece_slots),
             z_cols(lax.rem(chip, 2) * 2 + core),
         ]
 
@@ -643,40 +665,47 @@
         sends, recvs = (agp_send, agp_recv) if direction > 0 else (agm_send, agm_recv)
         view = sub_block(chip, h, c_me)
         return remote(
-            view, view, sends.at[h, k], recvs.at[h, k], tp=up if direction > 0 else down
+            view, view, sends, recvs.at[h, k], tp=up if direction > 0 else down
         )
 
     def across_copy(h, chip, core):
         view = sub_block(chip, h, core)
-        return remote(view, view, ags_send.at[h, chip], ags_recv.at[h, chip], tp=sibling)
+        return remote(view, view, ags_send, ags_recv.at[lax.div(chip, 2)], tp=sibling)
 
     def across_late(q, core):
         view = xg.at[q, :, x_cols(core)]
-        return remote(view, view, xf_send.at[q], xf_recv.at[q], tp=sibling)
+        return remote(view, view, ags_send, ags_recv.at[q], tp=sibling)
 
     def reach(direction, h):
-        return hops if (direction > 0) == (h == 0) else hops - 1
+        return hops if (direction > 0) == (h % 2 == 0) else hops - 1
 
     ahead_step(1)
     send_quad(quad_at(1))
     ahead_step(2)
     send_quad(quad_at(2))
-    for h in range(2):
-        for source in range(h * n_sp // 2, (h + 1) * n_sp // 2):
-
-            @pl.when(source != s_me)
-            def _(source=source):
-                dispatch_copy(0, source, source).wait_recv()
+    for h in range(PIECES):
+        group = n_sp // PIECES
+        mine = lax.div(s_me, group) == h
+
+        @pl.when(jnp.logical_not(mine))
+        def _(h=h, group=group):
+            got(og.at[:group], di_recv.at[h])
+
+        if group > 1:
+
+            @pl.when(mine)
+            def _(h=h, group=group):
+                got(og.at[: group - 1], di_recv.at[h])
 
         for direction in (1, -1):
             if reach(direction, h):
                 ring_copy(direction, h, 0, z_me).start()
         across_copy(h, z_me, c_me).start()
-    for load in loads[2:]:
-        load.wait()
+    pltpu.make_async_copy(wgu, wgu, load_sem.at[2]).wait()
+    pltpu.make_async_copy(wd, wd, load_sem.at[3]).wait()
 
     def forward(k, h):
-        for direction in (1, -1) if h == 0 else (-1, 1):
+        for direction in (1, -1) if h % 2 == 0 else (-1, 1):
             n = reach(direction, h)
 
             def arrive(direction=direction, n=n):
@@ -692,18 +721,14 @@
             pl.when(k <= n)(arrive)
 
     def forward_late(q):
-        def one(d, _):
-            late_copy(q, 0, sp_peer(d), sp_peer(d)).wait_recv()
-            return 0
-
-        lax.fori_loop(1, n_sp, one, 0)
+        got(ox.at[q, : n_sp - 1], ox_recv.at[q])
         across_late(q, c_me).start()
 
     def late_to_sibling(q):
         return remote(
             po.at[q, :, x_cols(1 - c_me)],
             xsib.at[q],
-            xsib_send.at[q],
+            xsib_send,
             xsib_recv.at[q],
             tp=sibling,
         )
@@ -712,15 +737,12 @@
         return [late_to_sibling(q)] + to_sibling(po, sib, sib_send, sib_recv, q, z_cols)
 
     def experts_gate(q):
-        for j in range(2):
-            for h in range(2):
-                across_copy(h, 2 * q + j, 1 - c_me).wait_recv()
-        across_late(q, 1 - c_me).wait_recv()
-        gs[...] = jax.nn.silu(jnp.dot(xg[q], wg[...], preferred_element_type=F32))
+        got(xg.at[q, :, : model // 2], ags_recv.at[q])
+        both = jnp.dot(xg[q], wgu[...], preferred_element_type=F32)
+        gs[...] = (jax.nn.silu(both[:, :units_n]) * both[:, units_n:]).astype(BF16)
 
     def experts(q):
-        up_part = jnp.dot(xg[q], wu[...], preferred_element_type=F32)
-        units = (gs[...] * up_part).astype(BF16)
+        units = gs[...]
         for part in range(PARTS):
             at = slice(part * width, (part + 1) * width)
             po[q, :, at] = jnp.dot(units, wd[:, at], preferred_element_type=F32).astype(BF16)
@@ -729,7 +751,7 @@
 
     def early_copy(q, d, source, peer):
         return remote(
-            xo.at[q, peer], xi.at[q, source], xo_send.at[q, d], xo_recv.at[q, source], sp=peer
+            xo.at[q, peer], xi.at[q, source], xo_send.at[q], xo_recv.at[q], sp=peer
         )
 
     def return_early(q):
@@ -749,49 +771,29 @@
             wl[q], back, preferred_element_type=F32
         )
 
+    def home_copy(chip):
+        return remote(
+            co.at[chip], ci.at[z_me], co_send, co_recv, tp=chip * 2 + c_me
+        )
+
+    def home_result():
+        got(ci.at[: n_z - 1], co_recv)
+        total = co[z_me].astype(F32)
+        for d in range(1, n_z):
+            total = total + ci[chip_at(d)].astype(F32)
+        return total
+
     def weigh_early(q):
-        def one(d, _):
-            early_copy(q, 0, sp_peer(d), sp_peer(d)).wait_recv()
-            return 0
-
-        lax.fori_loop(1, n_sp, one, 0)
+        got(xi.at[q, : n_sp - 1], xo_recv.at[q])
         total = weigh(q, xi[q].reshape(slots, width))
         for j in range(2):
-            co[2 * q + j] = total[:, j * half_w : (j + 1) * half_w]
-
-    def home_copy(direction, j, source):
-        sends, recvs, slot = (hp_send, hp_recv, hp) if direction > 0 else (hm_send, hm_recv, hm)
-        return remote(
-            source,
-            slot.at[j - 1],
-            sends.at[j - 1],
-            recvs.at[j - 1],
-            tp=up if direction > 0 else down,
-        )
-
-    ways = [(1, hops, hp), (-1, hops - 1, hm)]
-
-    def home_step(j):
-        for direction, n, slots_in in ways:
-            if j > n:
-                continue
-            value = co[chip_at(direction * (n + 1 - j))]
-            if j == 1:
-                source = hs_out.at[0 if direction > 0 else 1]
-            else:
-                source = slots_in.at[j - 2]
-                home_copy(direction, j - 1, source).wait_recv()
-                value = value + source[...].astype(F32)
-            source[...] = value.astype(BF16)
-            home_copy(direction, j, source).start()
-
-    def home_result():
-        total = co[z_me]
-        for direction, n, slots_in in ways:
-            if n:
-                home_copy(direction, n, slots_in.at[n - 1]).wait_recv()
-                total = total + slots_in[n - 1].astype(F32)
-        return total
+            chip = 2 * q + j
+            co[chip] = total[:, j * half_w : (j + 1) * half_w].astype(BF16)
+
+            @pl.when(chip != z_me)
+            def _(chip=chip):
+                home_copy(chip).start()
+
 
     def gather_step(k, _):
         @pl.when(k <= hops - 2)
@@ -801,7 +803,8 @@
 
         @pl.when(k <= hops)
         def _():
-            forward(k, 0)
+            for h in range(PIECES // 2):
+                forward(k, h)
 
         @pl.when(k >= 2)
         def _():
@@ -809,7 +812,8 @@
 
         @pl.when(k <= hops)
         def _():
-            forward(k, 1)
+            for h in range(PIECES // 2, PIECES):
+                forward(k, h)
             forward_late(quad_at(k))
 
         @pl.when(k >= 2)
@@ -830,42 +834,35 @@
         st,
         rp,
         rm,
-        (sib_send, sib_recv, rp_send, rp_recv, rm_send, rm_recv),
-        half_slots,
+        (sib_recv, rp_send, rp_recv, rm_send, rm_recv),
+        PIECES,
         z_cols,
     )
     begin()
     return_early(quad_at(hops))
 
-    homeward = 0
+    weighed = 0
     for j in range(2, hops + 1):
         step_of(j)
-        if homeward:
-            homeward += 1
-            home_step(homeward)
-        for k in range(2 * j - 3, min(2 * j - 1, hops + 1)):
+        upto = hops if j == hops else min(2 * j - 3, hops)
+        for k in range(weighed + 1, upto + 1):
             weigh_early(quad_at(k))
-            if k == hops:
-                homeward = 1
-                home_step(1)
-    half_sp = n_sp // 2
+        weighed = upto
+    piece_sp = n_sp // PIECES
 
     def return_copy(d, source, peer):
         return remote(
-            ret.at[peer], rt.at[source], ret_send.at[d], ret_recv.at[source], sp=peer
-        )
-
-    for h in range(2):
-        ret[h * half_sp : (h + 1) * half_sp] = (
-            result(h).astype(BF16).reshape(half_sp, slot_rows, half_w)
+            ret.at[peer], rt.at[source], ret_send, ret_recv, sp=peer
+        )
+
+    for h in range(PIECES):
+        ret[h * piece_sp : (h + 1) * piece_sp] = (
+            result(h).astype(BF16).reshape(piece_sp, slot_rows, half_w)
         )
     rt[pl.ds(s_me, 1)] = ret[pl.ds(s_me, 1)]
     for d in range(1, n_sp):
         return_copy(d, s_me, sp_peer(d)).start()
-    for j in range(homeward + 1, hops + 1):
-        home_step(j)
-    for d in range(1, n_sp):
-        return_copy(d, sp_peer(d), sp_peer(d)).wait_recv()
+    got(rt.at[: n_sp - 1], ret_recv)
     routed = weigh(q_me, rt[...].reshape(slots, half_w))
     fo[:, :, :half_w] = (
         (resid[:, :half_w].astype(F32) + routed)
@@ -884,52 +881,39 @@
         return remote(
             fo.at[peer],
             fin.at[source],
-            fin_send.at[d],
-            fin_recv.at[source],
+            fin_send,
+            fin_recv,
             tp=q_me * PARTS + peer,
         )
 
     for d in range(1, PARTS):
         final_copy(d, p_me, quad_peer(d)).start()
-    for d in range(1, PARTS):
-        final_copy(d, quad_peer(d), quad_peer(d)).wait_recv()
+    sent(rx.at[: (n_sp - 1) * 16, :], fr_send)
+    sent(sqb.at[: n_tp - 1], sq_send)
+    sent(psib, psib_send)
+    drain_projection()
+    sent(sq2.at[: PARTS - 1], s2_send)
+    sent(xa.at[:hops], xap_send)
+    if hops > 1:
+        sent(xa.at[: hops - 1], xam_send)
+    sent(og.at[: n_sp - 1], di_send)
+    hop_count = PIECES // 2 * (2 * hops - 1)
+    sent(rp.at[:hop_count], agp_send)
+    sent(rm.at[:hop_count], agm_send)
+    sent(xg.at[:2], ags_send) if quads == 4 else sent(xg, ags_send)
+    for q in range(quads):
+        sent(ox.at[q, : n_sp - 1], ox_send.at[q])
+        sent(xo.at[q, : n_sp - 1], xo_send.at[q])
+    sent(sib, sib_send)
+    sent(xsib, xsib_send)
+    drain_experts()
+    sent(co.at[: n_z - 1], co_send)
+    sent(ret.at[: n_sp - 1], ret_send)
+    got(fin.at[: PARTS - 1], fin_recv)
     for part in range(PARTS):
         out[:, part * width : (part + 1) * width] = fin[part]
-
-    for d in range(1, n_sp):
-        front_copy(d, s_me).wait_send()
-        dispatch_copy(d, s_me, sp_peer(d)).wait_send()
-        return_copy(d, s_me, sp_peer(d)).wait_send()
-    for d in range(1, n_tp):
-        square_copy(d, t_me).wait_send()
-    for d in range(1, PARTS):
-        norm_copy(d, p_me).wait_send()
-        final_copy(d, p_me, quad_peer(d)).wait_send()
-    for h in range(2):
-        for direction in (1, -1):
-            for k in range(reach(direction, h)):
-                ring_copy(direction, h, k, z_me).wait_send()
-        for chip in range(n_z):
-            across_copy(h, chip, c_me).wait_send()
-    for copy in copies:
-        copy.wait_send()
-    drain_projection()
-    drain_experts()
-    for direction, n, slots_in in ways:
-        for k in range(n):
-            ahead_copy(direction, k, z_me).wait_send()
-            home_copy(direction, k + 1, slots_in.at[k]).wait_send()
-    for q in range(quads):
-        across_late(q, c_me).wait_send()
-        for copy in out_to_sibling(q):
-            copy.wait_send()
-
-        def one(d, _, q=q):
-            late_copy(q, d, s_me, sp_peer(d)).wait_send()
-            early_copy(q, d, s_me, sp_peer(d)).wait_send()
-            return 0
-
-        lax.fori_loop(1, n_sp, one, 0)
+    sent(fo.at[: PARTS - 1], fin_send)
+
 
 def local(
     n_sp,
@@ -968,6 +952,18 @@
     hbm = pl.BlockSpec(memory_space=pl.ANY)
     dma = pltpu.SemaphoreType.DMA
     scratch = [
+        pltpu.VMEM(lru_input.shape, BF16),
+        pltpu.VMEM(gate_input.shape, BF16),
+        pltpu.VMEM((1, positions), jnp.int32),
+        pltpu.VMEM(conv_taps.shape, BF16),
+        pltpu.VMEM(rate_weight.shape[1:], BF16),
+        pltpu.VMEM(inlet_weight.shape[1:], BF16),
+        pltpu.VMEM((1, channels), F32),
+        pltpu.VMEM((1, channels), F32),
+        pltpu.VMEM((1, model), F32),
+        pltpu.VMEM((2, positions), jnp.int32),
+        pltpu.VMEM((2, positions), F32),
+        dma((11,)),
         pltpu.VMEM((positions + 8, LANES), F32),
         pltpu.VMEM((positions + 8, LANES), F32),
         pltpu.VMEM((pitch, LANES), F32),
@@ -978,16 +974,15 @@
         pltpu.VMEM((6 * n_sp, LANES), F32),
         pltpu.VMEM((channels, model), BF16),
         pltpu.VMEM((tokens, width), BF16),
-        pltpu.VMEM((model, units), BF16),
-        pltpu.VMEM((model, units), BF16),
+        pltpu.VMEM((model, 2 * units), BF16),
         pltpu.VMEM((units, model), BF16),
         pltpu.VMEM((n_tp, 1, positions), F32),
         pltpu.VMEM((PARTS, 1, LANES), F32),
         pltpu.VMEM((quads, tokens, model), BF16),
         pltpu.VMEM((n_z, tokens, width), BF16),
         pltpu.VMEM((4, tokens // 2, width), BF16),
-        pltpu.VMEM((2, hops, tokens // 2, width), BF16),
-        pltpu.VMEM((2, hops, tokens // 2, width), BF16),
+        pltpu.VMEM((2 * hops, tokens // 2, width), BF16),
+        pltpu.VMEM((2 * hops, tokens // 2, width), BF16),
         pltpu.VMEM((quads, tokens, block_rows), BF16),
         pltpu.VMEM((quads, tokens, block_rows), BF16),
         pltpu.VMEM((quads, tokens, block_rows), BF16),
@@ -1000,70 +995,64 @@
         pltpu.VMEM((quads, block_rows, width), BF16),
         pltpu.VMEM((quads, n_sp, slot_rows, width), BF16),
         pltpu.VMEM((quads, n_sp, slot_rows, width), BF16),
-        pltpu.VMEM((n_z, tokens, half_w), F32),
-        pltpu.VMEM((2, tokens, half_w), BF16),
-        pltpu.VMEM((hops, tokens, half_w), BF16),
-        pltpu.VMEM((hops, tokens, half_w), BF16),
-        pltpu.VMEM((block_rows, units), F32),
-        pltpu.VMEM((4, block_rows // 2, half_w), BF16),
-        pltpu.VMEM((2, hops, block_rows // 2, half_w), BF16),
-        pltpu.VMEM((2, hops, block_rows // 2, half_w), BF16),
+        pltpu.VMEM((n_z, tokens, half_w), BF16),
+        pltpu.VMEM((n_z, tokens, half_w), BF16),
+        pltpu.VMEM((block_rows, units), BF16),
+        pltpu.VMEM((2 * PIECES, block_rows // PIECES, half_w), BF16),
+        pltpu.VMEM((PIECES * hops, block_rows // PIECES, half_w), BF16),
+        pltpu.VMEM((PIECES * hops, block_rows // PIECES, half_w), BF16),
         pltpu.VMEM((n_sp, slot_rows, half_w), BF16),
         pltpu.VMEM((n_sp, slot_rows, half_w), BF16),
         pltpu.VMEM((PARTS, ROUTE_ROWS, width), BF16),
         pltpu.VMEM((PARTS, ROUTE_ROWS, width), BF16),
-        dma((2 + 6 * PARTS,)),
-        dma((n_sp,)),
-        dma((n_sp,)),
-        dma((n_tp,)),
-        dma((n_tp,)),
-        dma((PARTS,)),
-        dma((PARTS,)),
-        dma((n_z,)),
-        dma((n_z,)),
+        dma((4,)),
+        dma(()),
+        dma(()),
+        dma(()),
+        dma(()),
+        dma(()),
+        dma(()),
+        dma(()),
+        dma((quads,)),
+        dma(()),
         dma((2, hops)),
+        dma(()),
         dma((2, hops)),
-        dma((2, hops)),
-        dma((2, hops)),
-        dma((n_sp,)),
-        dma((n_sp,)),
-        dma((2, hops)),
-        dma((2, hops)),
-        dma((2, hops)),
-        dma((2, hops)),
-        dma((2, n_z)),
-        dma((2, n_z)),
+        dma(()),
+        dma((PIECES,)),
+        dma(()),
+        dma((PIECES, hops)),
+        dma(()),
+        dma((PIECES, hops)),
+        dma(()),
+        dma((quads,)),
+        dma(()),
         dma((hops,)),
+        dma(()),
         dma((hops,)),
-        dma((hops,)),
-        dma((hops,)),
-        dma((quads, n_sp)),
-        dma((quads, n_sp)),
         dma((quads,)),
         dma((quads,)),
-        dma((n_z,)),
-        dma((n_z,)),
+        dma(()),
+        dma((quads,)),
+        dma(()),
         dma((quads,)),
         dma((quads,)),
-        dma((quads, n_sp)),
-        dma((quads, n_sp)),
-        dma((hops,)),
-        dma((hops,)),
-        dma((hops,)),
-        dma((hops,)),
-        dma((2, hops)),
-        dma((2, hops)),
-        dma((2, hops)),
-        dma((2, hops)),
-        dma((n_sp,)),
-        dma((n_sp,)),
-        dma((PARTS,)),
-        dma((PARTS,)),
+        dma((quads,)),
+        dma(()),
+        dma(()),
+        dma(()),
+        dma((PIECES, hops)),
+        dma(()),
+        dma((PIECES, hops)),
+        dma(()),
+        dma(()),
+        dma(()),
+        dma(()),
     ]
     return pl.pallas_call(
         functools.partial(kernel, n_sp, n_tp),
         out_shape=jax.ShapeDtypeStruct((positions // n_tp, model), BF16),
-        in_specs=[vmem] * 11 + [hbm] * 5,
+        in_specs=[hbm] * 16,
         out_specs=vmem,
         scratch_shapes=scratch,
         name="layer",

time: 98.7 us -> 90 us (0.912)
  Pallas kernels: 97 us -> 88.4 us
    pallas_call x1, Pallas kernels: 97 us -> 88.4 us  [local(): pl.pallas_call(functools.partial(kernel, n_sp, n_tp), out_shape=jax.Shape...]
where the time goes in v3:
time: 90 us; the launch traced here: 89.9 us
  Pallas kernels  88.4 us (98%)
  local copies, waits for them, and re-layouts  1.47 us (2%)
    pallas_call x1, Pallas kernels, local(): pl.pallas_call(functools.partial(kernel, n_sp, n_tp), out_shape=jax.Shape...  88.4 us

profile of v3, /device:TPU:1, one launch (start us, length us, event | category | flops | bytes accessed | tf_op | source)
XLA Modules:
  0.0 89.9 jit_solution(14354177280518194275)
XLA Ops:
  0.0 88.4 %layer.1 = bf16[16,2048]{1,0:T(8,128)(2,1)} custom-call(bf16[256,128]{1,0:T(8,128)(2,1)} %lru_hbm.1, bf16[256,128]{1,0:T(8,128)(2,1)} %gate_hbm.1, s32[1,256]{1,0:T(1,128)} %bitcast.19, bf16[4,128]{1,0:T(4,128)(2,1)} %taps_hbm.1, bf16[128,128]{1,0:T(8,128)(2,1)} %bitcast.14, bf16[128,128]{1,0:T(8,128)(2,1)} %bitcast.15, f32[1,128]{1,0:T(1,128)} %bitcast.20, ...), custom_call_target="tpu_custom_call" | custom-call | tf_op jit(solution)/shard_map/layer/pallas_call | solution.py:1052
  88.4 1.5 %copy.18 = bf16[16,2048]{1,0:T(8,128)(2,1)} copy(bf16[16,2048]{1,0:T(8,128)(2,1)} %layer.1) | data formatting | bytes 131072
